TPU v7x, 32 devices: a whole 2x2x4 slice. The times are simulated.
32 devices in a mesh: fs: 8 (over z, y), tp: 4 (over x, core).
Axes of the slice: x: 2, y: 2, z: 4, core: 2. Of those that a mesh axis runs over, the one named last changes fastest.
Arguments:
- tokens: bfloat16 [3072, 2048], P('fs'), may hold values from -6 to 6
- first_norm_scale: float32 [2048], replicated, may hold values from 0.1 to 1.9
- recurrent_branch_matrix: bfloat16 [2048, 1024], P('fs', 'tp'), may hold values from -0.125 to 0.125
- gelu_gate_matrix: bfloat16 [2048, 1024], P('fs', 'tp'), may hold values from -0.125 to 0.125
- filter_taps_weight: bfloat16 [4, 1024], P(None, 'tp'), may hold values from -3 to 3
- recurrence_gate_blocks: bfloat16 [16, 64, 64], P('tp'), may hold values from -0.75 to 0.75
- input_gate_blocks: bfloat16 [16, 64, 64], P('tp'), may hold values from -0.75 to 0.75
- base_decay_logits: float32 [1024], P('tp'), may hold values from 4 to 11
- extra_log_decay: float32 [3072, 1024], P('fs', 'tp'), may hold values from -0.7 to 0
- mixer_output_matrix: bfloat16 [2048, 1024], P('fs', 'tp'), may hold values from -0.5 to 0.5
- second_norm_scale: float32 [2048], replicated, may hold values from 0.1 to 1.9
- mixer_up_matrix: bfloat16 [2048, 4096], P('fs', 'tp'), may hold values from -0.125 to 0.125
- mixer_down_matrix: bfloat16 [2048, 4096], P('fs', 'tp'), may hold values from -0.09375 to 0.09375
Outputs:
- layer_out: bfloat16 [3072, 2048], P(('fs', 'tp'))
All inputs are finite; a program needn't handle non-finite values.
Results may differ from a plain program's by a relative error of at most 0.022.
Values may be sent and summed in bfloat16 or wider, within the bound.
A program may use at most 64 MiB of HBM per device.

v0:
```python
import functools

import jax
import jax.numpy as jnp
from jax import lax
from jax.experimental import pallas as pl
from jax.experimental.pallas import tpu as pltpu
from jax.sharding import PartitionSpec as P

epsilon = 1e-06
decay_rate_scale = 8.0


def rms_scaled(sequence_token_rows, scales):
    widened = sequence_token_rows.astype(jnp.float32)
    mean_square = jnp.mean(widened * widened, axis=-1, keepdims=True)
    return (widened * lax.rsqrt(mean_square + epsilon) * scales).astype(jnp.bfloat16)


def linear_combine(earlier, later):
    return (earlier[0] * later[0], later[0] * earlier[1] + later[1])


def causal_taps(branch, filter_taps_weight):
    tap_count = filter_taps_weight.shape[0]
    positions = branch.shape[0]
    padded = jnp.pad(branch.astype(jnp.float32), ((tap_count - 1, 0), (0, 0)))
    running = jnp.zeros(branch.shape, jnp.float32)
    for offset in range(tap_count):
        running = running + padded[offset : offset + positions] * filter_taps_weight[offset].astype(
            jnp.float32
        )
    return running.astype(jnp.bfloat16)


def block_map(convolved, blocks):
    positions, channels = convolved.shape
    grouped = convolved.reshape(positions, blocks.shape[0], blocks.shape[1])
    mapped = jnp.einsum("sgi,gij->sgj", grouped, blocks, preferred_element_type=jnp.float32)
    return jax.nn.sigmoid(mapped.reshape(positions, channels))


def contract_columns(left, right):
    return lax.dot_general(
        left, right, (((1,), (1,)), ((), ())), preferred_element_type=jnp.float32
    )


def local(
    tokens,
    first_norm_scale,
    recurrent_branch_matrix,
    gelu_gate_matrix,
    filter_taps_weight,
    recurrence_gate_blocks,
    input_gate_blocks,
    base_decay_logits,
    extra_log_decay,
    mixer_output_matrix,
    second_norm_scale,
    mixer_up_matrix,
    mixer_down_matrix,
):
    positions = tokens.shape[0]
    own_count = positions // lax.axis_size("tp")
    normed = rms_scaled(tokens, first_norm_scale)
    branch_sum = jnp.dot(
        normed,
        lax.all_gather(recurrent_branch_matrix, "fs", axis=0, tiled=True),
        preferred_element_type=jnp.float32,
    )
    gate_sum = jnp.dot(
        normed,
        lax.all_gather(gelu_gate_matrix, "fs", axis=0, tiled=True),
        preferred_element_type=jnp.float32,
    )
    branch = branch_sum.astype(jnp.bfloat16)
    gate_branch = gate_sum.astype(jnp.bfloat16)
    out_full = lax.all_gather(mixer_output_matrix, "fs", axis=0, tiled=True)
    convolved = causal_taps(branch, filter_taps_weight)
    recurrence_gate_value = block_map(convolved, recurrence_gate_blocks)
    admission = block_map(convolved, input_gate_blocks)
    log_keep_factor = (
        decay_rate_scale * recurrence_gate_value * jax.nn.log_sigmoid(base_decay_logits)
        + extra_log_decay
    )
    retain = jnp.exp(log_keep_factor)
    driven = jnp.sqrt(-jnp.expm1(2.0 * log_keep_factor)) * (
        admission * convolved.astype(jnp.float32)
    )
    memory = lax.associative_scan(linear_combine, (retain, driven), axis=0)[1]
    recurrent = (memory * jax.nn.gelu(gate_branch.astype(jnp.float32))).astype(jnp.bfloat16)
    up_full = lax.all_gather(mixer_up_matrix, "fs", axis=0, tiled=True)
    whole_sum = lax.psum(contract_columns(recurrent, out_full).astype(jnp.bfloat16), "tp").astype(
        jnp.float32
    )
    residual_all = (tokens.astype(jnp.float32) + whole_sum).astype(jnp.bfloat16)
    raised = jnp.dot(
        rms_scaled(residual_all, second_norm_scale), up_full, preferred_element_type=jnp.float32
    )
    hidden = jnp.square(jax.nn.relu(raised)).astype(jnp.bfloat16)
    residual = lax.dynamic_slice_in_dim(
        residual_all, lax.axis_index("tp") * own_count, own_count, 0
    )
    down_full = lax.all_gather(mixer_down_matrix, "fs", axis=0, tiled=True)
    channel_sum = lax.psum_scatter(
        contract_columns(hidden, down_full).astype(jnp.bfloat16),
        "tp",
        scatter_dimension=0,
        tiled=True,
    ).astype(jnp.float32)
    return (residual.astype(jnp.float32) + channel_sum).astype(jnp.bfloat16)


MESH = pl.DeviceIdType.MESH
Y_SIZE = 2
GROUPS = 4


def fits(mesh):
    n_fs, n_tp = mesh.shape["fs"], mesh.shape["tp"]
    return n_tp == 2 * Y_SIZE and n_fs == 4 * Y_SIZE


def shifted_down(values, by, fill):
    if by % 8 == 0:
        top = jnp.full((by, values.shape[1]), fill, values.dtype)
        return jnp.concatenate([top, values[: values.shape[0] - by]], axis=0)
    rows = lax.broadcasted_iota(jnp.int32, values.shape, 0)
    return jnp.where(rows < by, fill, pltpu.roll(values, by, 0))


def one_minus_exp(exponent):
    series = 1.0
    for order in range(8, 1, -1):
        series = 1.0 + exponent * (1.0 / order) * series
    return jnp.where(exponent > -0.35, -exponent * series, 1.0 - jnp.exp(exponent))


def fused(
    nz,
    tok_in, scale1, wb, wg, taps, rblk, iblk, logits, extra_in, wo, scale2, wu, wd,
    out,
    normed, fb, fg, fo, fu, fd, rdiag, idiag,
    part, pair1, give2, got2, res, mid, hidden,
    part_f, pair_f, give_f, got_f,
    send_sem, recv_sem, a_send, a_recv, b_send, b_recv, l_sem, tok, extra,
):
    f = lax.axis_index("fs")
    t = lax.axis_index("tp")
    z, y = f // Y_SIZE, f % Y_SIZE
    x, c = t // 2, t % 2
    last = nz - 1
    ymate = z * Y_SIZE + (1 - y)
    xmate = (1 - x) * 2 + c
    cmate = x * 2 + (1 - c)
    rows, width = tok.shape
    own_rows = out.shape[0]
    depth = wb.shape[0]
    half = depth // 2

    early = [
        pltpu.make_async_copy(tok_in, tok, l_sem.at[5]),
        pltpu.make_async_copy(extra_in, extra, l_sem.at[6]),
    ]
    for copy in early:
        copy.start()
    barrier = pltpu.get_barrier_semaphore()
    zup = lax.rem(z + 1, nz) * Y_SIZE + y
    zdown = lax.rem(z + nz - 1, nz) * Y_SIZE + y
    for other in (zup, zdown, ymate):
        pl.semaphore_signal(barrier, inc=1, device_id={"fs": other, "tp": t}, device_id_type=MESH)
    for other in (xmate, cmate):
        pl.semaphore_signal(barrier, inc=1, device_id={"fs": f, "tp": other}, device_id_type=MESH)
    pl.semaphore_wait(barrier, 5)

    pieces = (
        (wb, fb, 0, depth, False),
        (wg, fg, 0, depth, False),
        (wo, fo, 0, depth, True),
        (wu, fu, 0, half, False),
        (wu, fu, half, half, True),
        (wd, fd, 0, half, False),
        (wd, fd, half, half, True),
    )
    sent = []

    def slot(g, shard):
        _, full, first, count, _ = pieces[g]
        return full.at[pl.ds(pl.multiple_of(shard * depth + first, half), count), :]

    def give(g, shard, way, pred, source=None):
        target = (zup, zdown, ymate)[way]
        here = slot(g, shard)
        copy = pltpu.make_async_remote_copy(
            src_ref=here if source is None else source,
            dst_ref=here,
            send_sem=send_sem.at[g, shard, way],
            recv_sem=recv_sem.at[g, shard],
            device_id={"fs": target, "tp": t},
            device_id_type=MESH,
        )
        if pred is None:
            copy.start()
            sent.append((None, copy))
        else:
            pl.when(pred)(copy.start)
            sent.append((pred, copy))

    def take(g, shard):
        here = slot(g, shard)
        pltpu.make_async_remote_copy(
            src_ref=here,
            dst_ref=here,
            send_sem=send_sem.at[g, shard, 0],
            recv_sem=recv_sem.at[g, shard],
            device_id={"fs": ymate, "tp": t},
            device_id_type=MESH,
        ).wait_recv()

    def own(g):
        w, _, first, count, _ = pieces[g]
        source = w.at[pl.ds(first, count), :]
        give(g, f, 0, z < last, source)
        give(g, f, 1, z > 0, source)
        give(g, f, 2, None, source)

    def wave(g, d):
        along = pieces[g][4]
        for way in (0, 1):
            edge = 0 if way == 0 else last
            zs = z - d if way == 0 else z + d
            exists = zs >= 0 if way == 0 else zs <= last
            onward = z < last if way == 0 else z > 0
            if d > 0:
                shard = zs * Y_SIZE + y
                pl.when(exists)(functools.partial(take, g, shard))
                give(g, shard, way, exists & onward)
                if along:
                    give(g, shard, 2, exists & (zs != 0) & (zs != last))
                else:
                    give(g, shard, 2, exists)
            if along:
                outer = zs == edge
                shard = edge * Y_SIZE + (1 - y)
                pl.when(outer)(functools.partial(take, g, shard))
                give(g, shard, way, outer & onward)

    def take_across(g):
        for zs in range(nz):
            if not (pieces[g][4] and zs in (0, last)):
                take(g, zs * Y_SIZE + (1 - y))

    def tp_copy(source, target, other, index, send, recv):
        return pltpu.make_async_remote_copy(
            src_ref=source,
            dst_ref=target,
            send_sem=send.at[index],
            recv_sem=recv.at[index],
            device_id={"fs": f, "tp": other},
            device_id_type=MESH,
        )

    own(0)
    own(1)
    own(2)

    place = pl.ds(pl.multiple_of(f * depth, depth), depth)
    stays = [
        pltpu.make_async_copy(w, full.at[place, :], l_sem.at[i])
        for i, (w, full) in enumerate(((wb, fb), (wg, fg), (wo, fo), (wu, fu), (wd, fd)))
    ]
    for copy in stays:
        copy.start()
    block = rblk.shape[1]
    for blocks, diag in ((rblk, rdiag), (iblk, idiag)):
        diag[...] = jnp.zeros_like(diag)
        for b in range(rblk.shape[0]):
            diag[b * block : (b + 1) * block, b * block : (b + 1) * block] = blocks[b]

    for copy in early:
        copy.wait()

    def norm_rows(i, carry):
        at = pl.ds(pl.multiple_of(i * 32, 32), 32)
        normed[at, :] = rms_scaled(tok[at, :], scale1[...])
        return carry

    lax.fori_loop(0, rows // 32, norm_rows, 0)

    wave(0, 1)
    wave(1, 1)
    own(3)
    wave(2, 0)
    wave(2, 1)
    wave(0, 2)
    wave(1, 2)
    own(4)
    wave(3, 1)
    wave(0, 3)
    wave(1, 3)
    wave(2, 2)
    own(5)
    take_across(0)
    take_across(1)
    for copy in stays:
        copy.wait()

    branch = jnp.dot(normed[...], fb[...], preferred_element_type=jnp.float32)
    branch = branch.astype(jnp.bfloat16).astype(jnp.float32)
    tap_count = taps.shape[0]
    running = branch * taps[tap_count - 1 : tap_count, :].astype(jnp.float32)
    for offset in range(tap_count - 1):
        by = tap_count - 1 - offset
        running = running + shifted_down(branch, by, 0.0) * taps[offset : offset + 1, :].astype(
            jnp.float32
        )
    convolved = running.astype(jnp.bfloat16)
    rate = jax.nn.sigmoid(jnp.dot(convolved, rdiag[...], preferred_element_type=jnp.float32))
    admission = jax.nn.sigmoid(jnp.dot(convolved, idiag[...], preferred_element_type=jnp.float32))
    base = -jnp.log1p(jnp.exp(-logits[...]))
    log_keep = decay_rate_scale * rate * base + extra[...]
    keep = jnp.exp(log_keep)
    memory = jnp.sqrt(one_minus_exp(2.0 * log_keep)) * (admission * convolved.astype(jnp.float32))
    by = 1
    while by < rows:
        memory = keep * shifted_down(memory, by, 0.0) + memory
        if 2 * by < rows:
            keep = keep * shifted_down(keep, by, 1.0)
        by *= 2
    gate = jnp.dot(normed[...], fg[...], preferred_element_type=jnp.float32)
    gate = gate.astype(jnp.bfloat16).astype(jnp.float32)
    recurrent = (memory * jax.nn.gelu(gate)).astype(jnp.bfloat16)

    wave(2, 3)
    wave(3, 2)
    own(6)
    take_across(2)
    for k in range(width // depth):
        product = contract_columns(recurrent, fo[k * depth : (k + 1) * depth, :])
        part[:, :, k * depth : (k + 1) * depth] = product.astype(jnp.bfloat16).reshape(
            part.shape[0], own_rows, depth
        )
    first = [
        tp_copy(part.at[2 * other + (1 - c)], pair1.at[other], cmate, other, a_send, a_recv)
        for other in range(2)
    ]
    for copy in first:
        copy.start()
    wave(4, 0)
    for copy in first:
        copy.wait_recv()
    away = part[2 * (1 - x) + c].astype(jnp.float32) + pair1[1 - x].astype(jnp.float32)
    give2[...] = away.astype(jnp.bfloat16)
    second = tp_copy(give2, got2, xmate, 2, a_send, a_recv)
    second.start()
    wave(4, 1)
    wave(3, 3)
    second.wait_recv()
    own_at = pl.ds(pl.multiple_of(t * own_rows, own_rows), own_rows)
    mixed = part[t].astype(jnp.float32) + pair1[x].astype(jnp.float32)
    mixed = mixed + got2[...].astype(jnp.float32)
    residual = (tok[own_at, :].astype(jnp.float32) + mixed).astype(jnp.bfloat16)
    res[...] = residual
    mid[t] = rms_scaled(residual, scale2[...])
    spread = [
        tp_copy(mid.at[t], mid.at[t], xmate, 3, a_send, a_recv),
        tp_copy(mid.at[t], mid.at[t], cmate, 4, a_send, a_recv),
    ]
    for copy in spread:
        copy.start()
    wave(4, 2)
    wave(5, 1)
    tp_copy(mid.at[xmate], mid.at[xmate], xmate, 3, a_send, a_recv).wait_recv()
    relay = tp_copy(mid.at[xmate], mid.at[xmate], cmate, 5, a_send, a_recv)
    relay.start()
    wave(4, 3)
    wave(5, 2)
    tp_copy(mid.at[cmate], mid.at[cmate], cmate, 4, a_send, a_recv).wait_recv()
    diagonal = (1 - x) * 2 + (1 - c)
    tp_copy(mid.at[diagonal], mid.at[diagonal], cmate, 5, a_send, a_recv).wait_recv()
    wave(6, 0)
    wave(6, 1)
    take_across(3)
    take_across(4)

    tile = 256

    def up_tile(i, carry):
        at = pl.ds(pl.multiple_of(i * tile, tile), tile)
        raised = jnp.dot(
            mid[...].reshape(rows, width), fu[:, at], preferred_element_type=jnp.float32
        )
        hidden[:, at] = jnp.square(jnp.maximum(raised, 0.0)).astype(jnp.bfloat16)
        return carry

    lax.fori_loop(0, fu.shape[1] // tile, up_tile, 0)

    span = width // GROUPS
    side = z // (nz // 2)
    inner = z + side * (last - 2 * z)
    ranks = [inner, 1 - inner] + list(range(2, nz))
    order = [rank + side * (last - 2 * rank) for rank in ranks]
    firsts, seconds = [], []

    def finish_first(j):
        for copy in firsts[j]:
            copy.wait_recv()
        away = part_f[j, 2 * (1 - x) + c].astype(jnp.float32) + pair_f[j, 1 - x].astype(jnp.float32)
        give_f[j] = away.astype(jnp.bfloat16)
        copy = tp_copy(give_f.at[j], got_f.at[j], xmate, 3 * j + 2, b_send, b_recv)
        copy.start()
        seconds.append(copy)

    def columns(j):
        return pl.ds(pl.multiple_of(order[j] * span, span), span)

    def finish_second(j):
        seconds[j].wait_recv()
        total = part_f[j, t].astype(jnp.float32) + pair_f[j, x].astype(jnp.float32)
        total = total + got_f[j].astype(jnp.float32)
        out[:, columns(j)] = (res[:, columns(j)].astype(jnp.float32) + total).astype(jnp.bfloat16)

    for j in range(GROUPS):
        if j == 1:
            wave(5, 3)
        if j > 1:
            wave(6, j)
        q = order[j]
        take(5, q * Y_SIZE + (1 - y))
        if j != last:
            pl.when((q != 0) & (q != last))(functools.partial(take, 6, q * Y_SIZE + (1 - y)))
        product = contract_columns(hidden[...], fd[columns(j), :])
        part_f[j] = product.astype(jnp.bfloat16).reshape(part.shape[0], own_rows, span)
        copies = [
            tp_copy(
                part_f.at[j, 2 * other + (1 - c)], pair_f.at[j, other], cmate, 3 * j + other,
                b_send, b_recv,
            )
            for other in range(2)
        ]
        for copy in copies:
            copy.start()
        firsts.append(copies)
        if j > 0:
            finish_first(j - 1)
        if j > 1:
            finish_second(j - 2)
    finish_first(GROUPS - 1)
    finish_second(GROUPS - 2)
    finish_second(GROUPS - 1)

    for pred, copy in sent:
        if pred is None:
            copy.wait_send()
        else:
            pl.when(pred)(copy.wait_send)
    for copy in first + [second] + spread + [relay] + seconds:
        copy.wait_send()
    for copies in firsts:
        for copy in copies:
            copy.wait_send()


def fused_local(
    mesh,
    tokens,
    first_norm_scale,
    recurrent_branch_matrix,
    gelu_gate_matrix,
    filter_taps_weight,
    recurrence_gate_blocks,
    input_gate_blocks,
    base_decay_logits,
    extra_log_decay,
    mixer_output_matrix,
    second_norm_scale,
    mixer_up_matrix,
    mixer_down_matrix,
):
    n_fs, n_tp = mesh.shape["fs"], mesh.shape["tp"]
    rows, width = tokens.shape
    own_rows = rows // n_tp
    channels = recurrent_branch_matrix.shape[1]
    units = mixer_up_matrix.shape[1]
    span = width // GROUPS
    low, high = jnp.bfloat16, jnp.float32
    vmem = pl.BlockSpec(memory_space=pltpu.VMEM)
    hbm = pl.BlockSpec(memory_space=pl.ANY)
    return pl.pallas_call(
        functools.partial(fused, n_fs // Y_SIZE),
        out_shape=jax.ShapeDtypeStruct((own_rows, width), low),
        in_specs=[hbm, vmem, hbm, hbm] + [vmem] * 4 + [hbm, hbm, vmem, hbm, hbm],
        out_specs=vmem,
        scratch_shapes=[
            pltpu.VMEM((rows, width), low),
            pltpu.VMEM((width, channels), low),
            pltpu.VMEM((width, channels), low),
            pltpu.VMEM((width, channels), low),
            pltpu.VMEM((width, units), low),
            pltpu.VMEM((width, units), low),
            pltpu.VMEM((channels, channels), low),
            pltpu.VMEM((channels, channels), low),
            pltpu.VMEM((n_tp, own_rows, width), low),
            pltpu.VMEM((2, own_rows, width), low),
            pltpu.VMEM((own_rows, width), low),
            pltpu.VMEM((own_rows, width), low),
            pltpu.VMEM((own_rows, width), low),
            pltpu.VMEM((n_tp, own_rows, width), low),
            pltpu.VMEM((rows, units), low),
            pltpu.VMEM((GROUPS, n_tp, own_rows, span), low),
            pltpu.VMEM((GROUPS, 2, own_rows, span), low),
            pltpu.VMEM((GROUPS, own_rows, span), low),
            pltpu.VMEM((GROUPS, own_rows, span), low),
            pltpu.SemaphoreType.DMA((7, n_fs, 3)),
            pltpu.SemaphoreType.DMA((7, n_fs)),
            pltpu.SemaphoreType.DMA((6,)),
            pltpu.SemaphoreType.DMA((6,)),
            pltpu.SemaphoreType.DMA((3 * GROUPS,)),
            pltpu.SemaphoreType.DMA((3 * GROUPS,)),
            pltpu.SemaphoreType.DMA((7,)),
            pltpu.VMEM((rows, width), low),
            pltpu.VMEM((rows, channels), high),
        ],
        compiler_params=pltpu.CompilerParams(
            collective_id=0, has_side_effects=True, vmem_limit_bytes=60 * 1024 * 1024
        ),
        name="fused_layer",
    )(
        tokens,
        first_norm_scale.reshape(1, width),
        recurrent_branch_matrix,
        gelu_gate_matrix,
        filter_taps_weight,
        recurrence_gate_blocks,
        input_gate_blocks,
        base_decay_logits.reshape(1, channels),
        extra_log_decay,
        mixer_output_matrix,
        second_norm_scale.reshape(1, width),
        mixer_up_matrix,
        mixer_down_matrix,
    )


def solution(mesh):
    in_specs = (
        P("fs", None),
        P(),
        P("fs", "tp"),
        P("fs", "tp"),
        P(None, "tp"),
        P("tp", None, None),
        P("tp", None, None),
        P("tp"),
        P("fs", "tp"),
        P("fs", "tp"),
        P(),
        P("fs", "tp"),
        P("fs", "tp"),
    )
    out_specs = P(("fs", "tp"), None)
    body = functools.partial(fused_local, mesh) if fits(mesh) else local
    return jax.shard_map(body, mesh=mesh, in_specs=in_specs, out_specs=out_specs, check_vma=False)
```

profile of v0, /device:TPU:0, one launch (start us, length us, event | category | flops | bytes accessed | tf_op | source)
XLA Modules:
  0.0 131.8 jit_solution(11497259537563426874)
XLA Ops:
  0.0 130.0 %fused_layer.1 = bf16[96,2048]{1,0:T(8,128)(2,1)} custom-call(bf16[384,2048]{1,0:T(8,128)(2,1)} %tok_in.1, f32[1,2048]{1,0:T(1,128)} %bitcast.3, bf16[256,256]{1,0:T(8,128)(2,1)} %wb.1, bf16[256,256]{1,0:T(8,128)(2,1)} %wg.1, bf16[4,256]{1,0:T(4,128)(2,1)} %taps.1, bf16[4,64,64]{2,1,0:T(8,128)(2,1)} %rblk.1, bf16[4,64,64]{2,1,0:T(8,128)(2,1)} %iblk.1, ...), custom_call_target="tpu_custom_call" | custom-call | tf_op jit(solution)/shard_map/fused_layer/pallas_call | solution.py:490
  130.0 1.8 %copy.15 = bf16[96,2048]{1,0:T(8,128)(2,1)} copy(bf16[96,2048]{1,0:T(8,128)(2,1)} %fused_layer.1) | data formatting | bytes 786432
where the time goes:
time: 132 us
  Pallas kernels  130 us (98%)
  local copies, waits for them, and re-layouts  1.77 us (1%)
    pallas_call x1, Pallas kernels, fused_local(): pl.pallas_call(functools.partial(fused, n_fs // Y_SIZE), out_shape=jax.Sh...  130 us

commit v1 on v0

v1 whole, which is shorter than its diff:
```python
import functools

import jax
import jax.numpy as jnp
from jax import lax
from jax.experimental import pallas as pl
from jax.experimental.pallas import tpu as pltpu
from jax.sharding import PartitionSpec as P

epsilon = 1e-06
decay_rate_scale = 8.0


def rms_scaled(sequence_token_rows, scales):
    widened = sequence_token_rows.astype(jnp.float32)
    mean_square = jnp.mean(widened * widened, axis=-1, keepdims=True)
    return (widened * lax.rsqrt(mean_square + epsilon) * scales).astype(jnp.bfloat16)


def linear_combine(earlier, later):
    return (earlier[0] * later[0], later[0] * earlier[1] + later[1])


def causal_taps(branch, filter_taps_weight):
    tap_count = filter_taps_weight.shape[0]
    positions = branch.shape[0]
    padded = jnp.pad(branch.astype(jnp.float32), ((tap_count - 1, 0), (0, 0)))
    running = jnp.zeros(branch.shape, jnp.float32)
    for offset in range(tap_count):
        running = running + padded[offset : offset + positions] * filter_taps_weight[offset].astype(
            jnp.float32
        )
    return running.astype(jnp.bfloat16)


def block_map(convolved, blocks):
    positions, channels = convolved.shape
    grouped = convolved.reshape(positions, blocks.shape[0], blocks.shape[1])
    mapped = jnp.einsum("sgi,gij->sgj", grouped, blocks, preferred_element_type=jnp.float32)
    return jax.nn.sigmoid(mapped.reshape(positions, channels))


def contract_columns(left, right):
    return lax.dot_general(
        left, right, (((1,), (1,)), ((), ())), preferred_element_type=jnp.float32
    )


def local(
    tokens,
    first_norm_scale,
    recurrent_branch_matrix,
    gelu_gate_matrix,
    filter_taps_weight,
    recurrence_gate_blocks,
    input_gate_blocks,
    base_decay_logits,
    extra_log_decay,
    mixer_output_matrix,
    second_norm_scale,
    mixer_up_matrix,
    mixer_down_matrix,
):
    positions = tokens.shape[0]
    own_count = positions // lax.axis_size("tp")
    normed = rms_scaled(tokens, first_norm_scale)
    branch_sum = jnp.dot(
        normed,
        lax.all_gather(recurrent_branch_matrix, "fs", axis=0, tiled=True),
        preferred_element_type=jnp.float32,
    )
    gate_sum = jnp.dot(
        normed,
        lax.all_gather(gelu_gate_matrix, "fs", axis=0, tiled=True),
        preferred_element_type=jnp.float32,
    )
    branch = branch_sum.astype(jnp.bfloat16)
    gate_branch = gate_sum.astype(jnp.bfloat16)
    out_full = lax.all_gather(mixer_output_matrix, "fs", axis=0, tiled=True)
    convolved = causal_taps(branch, filter_taps_weight)
    recurrence_gate_value = block_map(convolved, recurrence_gate_blocks)
    admission = block_map(convolved, input_gate_blocks)
    log_keep_factor = (
        decay_rate_scale * recurrence_gate_value * jax.nn.log_sigmoid(base_decay_logits)
        + extra_log_decay
    )
    retain = jnp.exp(log_keep_factor)
    driven = jnp.sqrt(-jnp.expm1(2.0 * log_keep_factor)) * (
        admission * convolved.astype(jnp.float32)
    )
    memory = lax.associative_scan(linear_combine, (retain, driven), axis=0)[1]
    recurrent = (memory * jax.nn.gelu(gate_branch.astype(jnp.float32))).astype(jnp.bfloat16)
    up_full = lax.all_gather(mixer_up_matrix, "fs", axis=0, tiled=True)
    whole_sum = lax.psum(contract_columns(recurrent, out_full).astype(jnp.bfloat16), "tp").astype(
        jnp.float32
    )
    residual_all = (tokens.astype(jnp.float32) + whole_sum).astype(jnp.bfloat16)
    raised = jnp.dot(
        rms_scaled(residual_all, second_norm_scale), up_full, preferred_element_type=jnp.float32
    )
    hidden = jnp.square(jax.nn.relu(raised)).astype(jnp.bfloat16)
    residual = lax.dynamic_slice_in_dim(
        residual_all, lax.axis_index("tp") * own_count, own_count, 0
    )
    down_full = lax.all_gather(mixer_down_matrix, "fs", axis=0, tiled=True)
    channel_sum = lax.psum_scatter(
        contract_columns(hidden, down_full).astype(jnp.bfloat16),
        "tp",
        scatter_dimension=0,
        tiled=True,
    ).astype(jnp.float32)
    return (residual.astype(jnp.float32) + channel_sum).astype(jnp.bfloat16)


MESH = pl.DeviceIdType.MESH
Y_SIZE = 2
MIX_GROUPS = 4
DOWN_GROUPS = 8


def fits(mesh):
    n_fs, n_tp = mesh.shape["fs"], mesh.shape["tp"]
    return n_tp == 2 * Y_SIZE and n_fs == 4 * Y_SIZE


def shifted_down(values, by, fill):
    if by % 8 == 0:
        top = jnp.full((by, values.shape[1]), fill, values.dtype)
        return jnp.concatenate([top, values[: values.shape[0] - by]], axis=0)
    rows = lax.broadcasted_iota(jnp.int32, values.shape, 0)
    return jnp.where(rows < by, fill, pltpu.roll(values, by, 0))


def one_minus_exp(exponent):
    series = 1.0
    for order in range(8, 1, -1):
        series = 1.0 + exponent * (1.0 / order) * series
    return jnp.where(exponent > -0.35, -exponent * series, 1.0 - jnp.exp(exponent))


def fused(
    nz,
    tok_in, scale1, wb, wg, taps, rblk, iblk, logits, extra_in, wo, scale2, wu, wd,
    out,
    normed, fb, fg, fo, fu, fd, rdiag, idiag, tok, extra,
    part1, pair1, give1, got1, res, mid, hidden,
    part2, pair2, xgive, xgot, zgive, zgot,
    z_send, y_send, w_recv, r_send, r_recv, a_send, a_recv, b_send, b_recv, l_sem,
):
    f = lax.axis_index("fs")
    t = lax.axis_index("tp")
    z, y = f // Y_SIZE, f % Y_SIZE
    x, c = t // 2, t % 2
    last = nz - 1
    parity = z % 2
    zmate = z + 1 - 2 * parity
    ymate = z * Y_SIZE + (1 - y)
    xmate = (1 - x) * 2 + c
    cmate = x * 2 + (1 - c)
    diagonal = (1 - x) * 2 + (1 - c)
    rows, width = tok.shape
    own_rows = out.shape[0]
    depth = wb.shape[0]
    half = depth // 2
    units = fu.shape[1]

    early = [
        pltpu.make_async_copy(tok_in, tok, l_sem.at[0]),
        pltpu.make_async_copy(extra_in, extra, l_sem.at[1]),
    ]
    for copy in early:
        copy.start()
    barrier = pltpu.get_barrier_semaphore()
    for k in range(1, nz):
        other = lax.rem(z + k, nz) * Y_SIZE + y
        pl.semaphore_signal(barrier, inc=1, device_id={"fs": other, "tp": t}, device_id_type=MESH)
    pl.semaphore_signal(barrier, inc=1, device_id={"fs": ymate, "tp": t}, device_id_type=MESH)
    for other in (xmate, cmate):
        pl.semaphore_signal(barrier, inc=1, device_id={"fs": f, "tp": other}, device_id_type=MESH)
    pl.semaphore_wait(barrier, nz + 2)

    sent = []

    def start(pred, copy):
        if pred is None:
            copy.start()
        else:
            pl.when(pred)(copy.start)
        sent.append((pred, copy))

    plain = (wb, wg, wo)
    whole = (fb, fg, fo)

    def source(g, way_parity):
        if g < 3:
            return plain[g]
        w = wu if g < 5 else wd
        first = half * ((g - 3) % 2)
        return w.at[
            pl.ds(first, half), pl.ds(pl.multiple_of(way_parity * units, units), units)
        ]

    def slot(g, zs, ys):
        if g < 3:
            return whole[g].at[pl.ds(pl.multiple_of((zs * Y_SIZE + ys) * depth, depth), depth), :]
        if g < 5:
            at = (zs * Y_SIZE + ys) * depth + (g - 3) * half
            return fu.at[pl.ds(pl.multiple_of(at, half), half), :]
        at = ((zs * 2 + (g - 5)) * Y_SIZE + ys) * half
        return fd.at[pl.ds(pl.multiple_of(at, half), half), :]

    def z_copy(g, src, zs, zt, index):
        return pltpu.make_async_remote_copy(
            src_ref=src,
            dst_ref=slot(g, zs, y),
            send_sem=z_send.at[g, index],
            recv_sem=w_recv.at[g, zs * Y_SIZE + y],
            device_id={"fs": zt * Y_SIZE + y, "tp": t},
            device_id_type=MESH,
        )

    def y_copy(g, src, zs):
        return pltpu.make_async_remote_copy(
            src_ref=src,
            dst_ref=slot(g, zs, y),
            send_sem=y_send.at[g, zs],
            recv_sem=w_recv.at[g, zs * Y_SIZE + y],
            device_id={"fs": ymate, "tp": t},
            device_id_type=MESH,
        )

    def take(g, zs, ys):
        here = slot(g, zs, ys)
        pltpu.make_async_remote_copy(
            src_ref=here,
            dst_ref=here,
            send_sem=y_send.at[g, zs],
            recv_sem=w_recv.at[g, zs * Y_SIZE + ys],
            device_id={"fs": ymate, "tp": t},
            device_id_type=MESH,
        ).wait_recv()

    def spread_z(g):
        for d in range(1, 2 if g < 3 else nz):
            for way in (0, 1):
                zt = z + d if way == 0 else z - d
                exists = zt <= last if way == 0 else zt >= 0
                start(exists, z_copy(g, source(g, lax.rem(zt + nz, 2)), z, zt, (d - 1) * 2 + way))

    def own(g):
        start(None, y_copy(g, source(g, parity), z))

    def forward(g, d):
        for way in (0, 1):
            zs = z - d if way == 0 else z + d
            exists = zs >= 0 if way == 0 else zs <= last
            pl.when(exists)(functools.partial(take, g, zs, y))
            if g < 3 and d < last:
                onward = z < last if way == 0 else z > 0
                zt = z + 1 if way == 0 else z - 1
                start(exists & onward, z_copy(g, slot(g, zs, y), zs, zt, d * 2 + way))
            start(exists, y_copy(g, slot(g, zs, y), zs))

    def take_across(g):
        for zs in range(nz):
            take(g, zs, 1 - y)

    def near_copy(src, dst, device, index, send, recv):
        copy = pltpu.make_async_remote_copy(
            src_ref=src,
            dst_ref=dst,
            send_sem=send.at[index],
            recv_sem=recv.at[index],
            device_id=device,
            device_id_type=MESH,
        )
        copy.start()
        sent.append((None, copy))
        return copy

    to_x = {"fs": f, "tp": xmate}
    to_c = {"fs": f, "tp": cmate}
    to_z = {"fs": zmate * Y_SIZE + y, "tp": t}

    spread_z(0)
    own(0)
    spread_z(1)
    own(1)

    stays = [
        pltpu.make_async_copy(source(g, parity), slot(g, z, y), l_sem.at[2 + g]) for g in range(7)
    ]
    for copy in stays:
        copy.start()
    block = rblk.shape[1]
    for blocks, diag in ((rblk, rdiag), (iblk, idiag)):
        diag[...] = jnp.zeros_like(diag)
        for b in range(rblk.shape[0]):
            diag[b * block : (b + 1) * block, b * block : (b + 1) * block] = blocks[b]

    for copy in early:
        copy.wait()

    def norm_rows(i, carry):
        at = pl.ds(pl.multiple_of(i * 32, 32), 32)
        normed[at, :] = rms_scaled(tok[at, :], scale1[...])
        return carry

    lax.fori_loop(0, rows // 32, norm_rows, 0)

    forward(0, 1)
    forward(1, 1)
    spread_z(2)
    forward(0, 2)
    own(2)
    forward(1, 2)
    forward(0, 3)
    forward(1, 3)
    forward(2, 1)
    forward(2, 2)
    spread_z(3)
    own(3)
    forward(2, 3)
    spread_z(4)
    spread_z(5)
    for copy in stays:
        copy.wait()
    take_across(0)

    branch = jnp.dot(normed[...], fb[...], preferred_element_type=jnp.float32)
    branch = branch.astype(jnp.bfloat16).astype(jnp.float32)
    tap_count = taps.shape[0]
    running = branch * taps[tap_count - 1 : tap_count, :].astype(jnp.float32)
    for offset in range(tap_count - 1):
        by = tap_count - 1 - offset
        running = running + shifted_down(branch, by, 0.0) * taps[offset : offset + 1, :].astype(
            jnp.float32
        )
    convolved = running.astype(jnp.bfloat16)
    rate = jax.nn.sigmoid(jnp.dot(convolved, rdiag[...], preferred_element_type=jnp.float32))
    admission = jax.nn.sigmoid(jnp.dot(convolved, idiag[...], preferred_element_type=jnp.float32))
    base = -jnp.log1p(jnp.exp(-logits[...]))
    log_keep = decay_rate_scale * rate * base + extra[...]
    keep = jnp.exp(log_keep)
    memory = jnp.sqrt(one_minus_exp(2.0 * log_keep)) * (admission * convolved.astype(jnp.float32))
    by = 1
    while by < rows:
        memory = keep * shifted_down(memory, by, 0.0) + memory
        if 2 * by < rows:
            keep = keep * shifted_down(keep, by, 1.0)
        by *= 2
    take_across(1)
    gate = jnp.dot(normed[...], fg[...], preferred_element_type=jnp.float32)
    gate = gate.astype(jnp.bfloat16).astype(jnp.float32)
    recurrent = (memory * jax.nn.gelu(gate)).astype(jnp.bfloat16)

    own(4)
    forward(3, 1)

    side = z // (nz // 2)
    inner = z + side * (last - 2 * z)
    ranks = [inner, 1 - inner] + list(range(2, nz))
    order = [rank + side * (last - 2 * rank) for rank in ranks]
    span = width // MIX_GROUPS
    own_at = pl.ds(pl.multiple_of(t * own_rows, own_rows), own_rows)
    firsts, seconds = [], []

    def mix_columns(j):
        return pl.ds(pl.multiple_of(order[j] * span, span), span)

    def mix_first(j):
        firsts[j].wait_recv()
        away = part1[j, 1 - x, c].astype(jnp.float32) + pair1[j, 1 - x].astype(jnp.float32)
        give1[j] = away.astype(jnp.bfloat16)
        seconds.append(
            near_copy(give1.at[j], got1.at[j], to_x, MIX_GROUPS + j, r_send, r_recv)
        )

    def mix_second(j):
        seconds[j].wait_recv()
        mixed = part1[j, x, c].astype(jnp.float32) + pair1[j, x].astype(jnp.float32)
        mixed = mixed + got1[j].astype(jnp.float32)
        at = mix_columns(j)
        res[:, at] = (tok[own_at, at].astype(jnp.float32) + mixed).astype(jnp.bfloat16)

    for j in range(MIX_GROUPS):
        take(2, order[j], 1 - y)
        product = contract_columns(recurrent, fo[mix_columns(j), :])
        part1[j] = product.astype(jnp.bfloat16).reshape(2, 2, own_rows, span)
        firsts.append(
            near_copy(part1.at[j, :, 1 - c], pair1.at[j], to_c, j, r_send, r_recv)
        )
        if j > 0:
            mix_first(j - 1)
        if j > 1:
            mix_second(j - 2)
    mix_first(MIX_GROUPS - 1)
    forward(4, 1)
    forward(3, 2)
    mix_second(MIX_GROUPS - 2)
    mix_second(MIX_GROUPS - 1)

    mid[parity, t] = rms_scaled(res[...], scale2[...])
    mine = mid.at[parity, t]
    theirs = mid.at[1 - parity, t]
    near_copy(mine, mine, to_x, 1, a_send, a_recv)
    near_copy(mine, mine, to_z, 0, a_send, a_recv)
    near_copy(mine, mine, to_c, 2, a_send, a_recv)
    spread_z(6)

    def arrived(par, who, index):
        here = mid.at[par, who]
        pltpu.make_async_remote_copy(
            src_ref=here,
            dst_ref=here,
            send_sem=a_send.at[index],
            recv_sem=a_recv.at[index],
            device_id=to_c,
            device_id_type=MESH,
        ).wait_recv()
        return here

    forward(4, 2)
    forward(3, 3)
    forward(4, 3)
    own(5)
    arrived(1 - parity, t, 0)
    near_copy(theirs, theirs, to_x, 3, a_send, a_recv)
    near_copy(theirs, theirs, to_c, 4, a_send, a_recv)
    beside = arrived(parity, xmate, 1)
    near_copy(beside, beside, to_c, 5, a_send, a_recv)
    own(6)
    forward(5, 1)
    arrived(parity, cmate, 2)
    arrived(parity, diagonal, 5)
    take_across(3)
    take_across(4)

    tile = 256

    def up(par):
        def up_tile(i, carry):
            at = pl.ds(pl.multiple_of(i * tile, tile), tile)
            raised = jnp.dot(
                mid[par].reshape(rows, width), fu[:, at], preferred_element_type=jnp.float32
            )
            hidden[par, :, at] = jnp.square(jnp.maximum(raised, 0.0)).astype(jnp.bfloat16)
            return carry

        lax.fori_loop(0, units // tile, up_tile, 0)

    up(parity)
    forward(6, 1)
    forward(5, 2)
    beside = arrived(1 - parity, xmate, 3)
    near_copy(beside, beside, to_c, 6, a_send, a_recv)
    arrived(1 - parity, cmate, 4)
    arrived(1 - parity, diagonal, 6)
    up(1 - parity)

    narrow = width // DOWN_GROUPS
    exchanges = [[], [], []]

    def place(j):
        return j // 2 + side * (last - 2 * (j // 2))

    def down_first(j):
        exchanges[0][j].wait_recv()
        for par in range(2):
            away = part2[j, par, 1 - x, c].astype(jnp.float32)
            away = away + pair2[j, par, 1 - x].astype(jnp.float32)
            xgive[j, par] = away.astype(jnp.bfloat16)
        exchanges[1].append(
            near_copy(xgive.at[j], xgot.at[j], to_x, DOWN_GROUPS + j, b_send, b_recv)
        )

    def partial_sum(j, par):
        total = part2[j, par, x, c].astype(jnp.float32) + pair2[j, par, x].astype(jnp.float32)
        return total + xgot[j, par].astype(jnp.float32)

    def down_second(j):
        exchanges[1][j].wait_recv()
        zgive[j] = partial_sum(j, 1 - parity).astype(jnp.bfloat16)
        exchanges[2].append(
            near_copy(zgive.at[j], zgot.at[j], to_z, 2 * DOWN_GROUPS + j, b_send, b_recv)
        )

    def down_third(j):
        exchanges[2][j].wait_recv()
        total = partial_sum(j, parity) + zgot[j].astype(jnp.float32)
        for ys in range(Y_SIZE):
            first = (place(j) * Y_SIZE + ys) * depth + (j % 2) * half
            at = pl.ds(pl.multiple_of(first, half), half)
            out[:, at] = (
                res[:, at].astype(jnp.float32) + total[:, ys * half : (ys + 1) * half]
            ).astype(jnp.bfloat16)

    ahead = {0: [(6, 2), (5, 3)], 1: [(6, 3)]}
    for j in range(DOWN_GROUPS):
        for g, d in ahead.get(j, []):
            forward(g, d)
        q = place(j)
        take(5 + j % 2, q, 1 - y)
        at = pl.ds(pl.multiple_of((q * 2 + j % 2) * narrow, narrow), narrow)
        product = contract_columns(hidden[...].reshape(2 * rows, units), fd[at, :])
        part2[j] = product.astype(jnp.bfloat16).reshape(2, 2, 2, own_rows, narrow)
        exchanges[0].append(
            near_copy(part2.at[j, :, :, 1 - c], pair2.at[j], to_c, j, b_send, b_recv)
        )
        if j > 0:
            down_first(j - 1)
        if j > 1:
            down_second(j - 2)
        if j > 2:
            down_third(j - 3)
    down_first(DOWN_GROUPS - 1)
    down_second(DOWN_GROUPS - 2)
    down_third(DOWN_GROUPS - 3)
    down_second(DOWN_GROUPS - 1)
    down_third(DOWN_GROUPS - 2)
    down_third(DOWN_GROUPS - 1)

    for pred, copy in sent:
        if pred is None:
            copy.wait_send()
        else:
            pl.when(pred)(copy.wait_send)


def fused_local(
    mesh,
    tokens,
    first_norm_scale,
    recurrent_branch_matrix,
    gelu_gate_matrix,
    filter_taps_weight,
    recurrence_gate_blocks,
    input_gate_blocks,
    base_decay_logits,
    extra_log_decay,
    mixer_output_matrix,
    second_norm_scale,
    mixer_up_matrix,
    mixer_down_matrix,
):
    n_fs, n_tp = mesh.shape["fs"], mesh.shape["tp"]
    rows, width = tokens.shape
    own_rows = rows // n_tp
    channels = recurrent_branch_matrix.shape[1]
    units = mixer_up_matrix.shape[1] // 2
    span = width // MIX_GROUPS
    narrow = width // DOWN_GROUPS
    low, high = jnp.bfloat16, jnp.float32
    vmem = pl.BlockSpec(memory_space=pltpu.VMEM)
    hbm = pl.BlockSpec(memory_space=pl.ANY)
    return pl.pallas_call(
        functools.partial(fused, n_fs // Y_SIZE),
        out_shape=jax.ShapeDtypeStruct((own_rows, width), low),
        in_specs=[hbm, vmem, hbm, hbm] + [vmem] * 4 + [hbm, hbm, vmem, hbm, hbm],
        out_specs=vmem,
        scratch_shapes=[
            pltpu.VMEM((rows, width), low),
            pltpu.VMEM((width, channels), low),
            pltpu.VMEM((width, channels), low),
            pltpu.VMEM((width, channels), low),
            pltpu.VMEM((width, units), low),
            pltpu.VMEM((width, units), low),
            pltpu.VMEM((channels, channels), low),
            pltpu.VMEM((channels, channels), low),
            pltpu.VMEM((rows, width), low),
            pltpu.VMEM((rows, channels), high),
            pltpu.VMEM((MIX_GROUPS, 2, 2, own_rows, span), low),
            pltpu.VMEM((MIX_GROUPS, 2, own_rows, span), low),
            pltpu.VMEM((MIX_GROUPS, own_rows, span), low),
            pltpu.VMEM((MIX_GROUPS, own_rows, span), low),
            pltpu.VMEM((own_rows, width), low),
            pltpu.VMEM((2, n_tp, own_rows, width), low),
            pltpu.VMEM((2, rows, units), low),
            pltpu.VMEM((DOWN_GROUPS, 2, 2, 2, own_rows, narrow), low),
            pltpu.VMEM((DOWN_GROUPS, 2, 2, own_rows, narrow), low),
            pltpu.VMEM((DOWN_GROUPS, 2, own_rows, narrow), low),
            pltpu.VMEM((DOWN_GROUPS, 2, own_rows, narrow), low),
            pltpu.VMEM((DOWN_GROUPS, own_rows, narrow), low),
            pltpu.VMEM((DOWN_GROUPS, own_rows, narrow), low),
            pltpu.SemaphoreType.DMA((7, 6)),
            pltpu.SemaphoreType.DMA((7, n_fs // Y_SIZE)),
            pltpu.SemaphoreType.DMA((7, n_fs)),
            pltpu.SemaphoreType.DMA((2 * MIX_GROUPS,)),
            pltpu.SemaphoreType.DMA((2 * MIX_GROUPS,)),
            pltpu.SemaphoreType.DMA((7,)),
            pltpu.SemaphoreType.DMA((7,)),
            pltpu.SemaphoreType.DMA((3 * DOWN_GROUPS,)),
            pltpu.SemaphoreType.DMA((3 * DOWN_GROUPS,)),
            pltpu.SemaphoreType.DMA((9,)),
        ],
        compiler_params=pltpu.CompilerParams(
            collective_id=0, has_side_effects=True, vmem_limit_bytes=60 * 1024 * 1024
        ),
        name="fused_layer",
    )(
        tokens,
        first_norm_scale.reshape(1, width),
        recurrent_branch_matrix,
        gelu_gate_matrix,
        filter_taps_weight,
        recurrence_gate_blocks,
        input_gate_blocks,
        base_decay_logits.reshape(1, channels),
        extra_log_decay,
        mixer_output_matrix,
        second_norm_scale.reshape(1, width),
        mixer_up_matrix,
        mixer_down_matrix,
    )


def solution(mesh):
    in_specs = (
        P("fs", None),
        P(),
        P("fs", "tp"),
        P("fs", "tp"),
        P(None, "tp"),
        P("tp", None, None),
        P("tp", None, None),
        P("tp"),
        P("fs", "tp"),
        P("fs", "tp"),
        P(),
        P("fs", "tp"),
        P("fs", "tp"),
    )
    out_specs = P(("fs", "tp"), None)
    body = functools.partial(fused_local, mesh) if fits(mesh) else local
    return jax.shard_map(body, mesh=mesh, in_specs=in_specs, out_specs=out_specs, check_vma=False)
```

time: 132 us -> 113 us (0.86)
  Pallas kernels: 130 us -> 111 us
    pallas_call x1, Pallas kernels: 130 us -> 111 us  [fused_local(): pl.pallas_call(functools.partial(fused, n_fs // Y_SIZE), out_shape=jax.Sh...]
where the time goes in v1:
time: 113 us
  Pallas kernels  111 us (98%)
  local copies, waits for them, and re-layouts  1.77 us (2%)
    pallas_call x1, Pallas kernels, fused_local(): pl.pallas_call(functools.partial(fused, n_fs // Y_SIZE), out_shape=jax.Sh...  111 us

profile of v1, /device:TPU:0, one launch (start us, length us, event | category | flops | bytes accessed | tf_op | source)
XLA Modules:
  0.0 113.0 jit_solution(9355251740362797226)
XLA Ops:
  0.0 111.2 %fused_layer.1 = bf16[96,2048]{1,0:T(8,128)(2,1)} custom-call(bf16[384,2048]{1,0:T(8,128)(2,1)} %tok_in.1, f32[1,2048]{1,0:T(1,128)} %bitcast.3, bf16[256,256]{1,0:T(8,128)(2,1)} %wb.1, bf16[256,256]{1,0:T(8,128)(2,1)} %wg.1, bf16[4,256]{1,0:T(4,128)(2,1)} %taps.1, bf16[4,64,64]{2,1,0:T(8,128)(2,1)} %rblk.1, bf16[4,64,64]{2,1,0:T(8,128)(2,1)} %iblk.1, ...), custom_call_target="tpu_custom_call" | custom-call | tf_op jit(solution)/shard_map/fused_layer/pallas_call | solution.py:556
  111.2 1.8 %copy.15 = bf16[96,2048]{1,0:T(8,128)(2,1)} copy(bf16[96,2048]{1,0:T(8,128)(2,1)} %fused_layer.1) | data formatting | bytes 786432

commit v2 on v1

--- a/solution.py
+++ b/solution.py
@@ -116,6 +116,7 @@
 Y_SIZE = 2
 MIX_GROUPS = 4
 DOWN_GROUPS = 8
+DIRECT = (7,)
 
 
 def fits(mesh):
@@ -144,7 +145,7 @@
     out,
     normed, fb, fg, fo, fu, fd, rdiag, idiag, tok, extra,
     part1, pair1, give1, got1, res, mid, hidden,
-    part2, pair2, xgive, xgot, zgive, zgot,
+    part2, pair2, agive, agot, bgive, bgot,
     z_send, y_send, w_recv, r_send, r_recv, a_send, a_recv, b_send, b_recv, l_sem,
 ):
     f = lax.axis_index("fs")
@@ -153,6 +154,7 @@
     x, c = t // 2, t % 2
     last = nz - 1
     parity = z % 2
+    at_end = (z == 0) | (z == last)
     zmate = z + 1 - 2 * parity
     ymate = z * Y_SIZE + (1 - y)
     xmate = (1 - x) * 2 + c
@@ -177,7 +179,9 @@
     pl.semaphore_signal(barrier, inc=1, device_id={"fs": ymate, "tp": t}, device_id_type=MESH)
     for other in (xmate, cmate):
         pl.semaphore_signal(barrier, inc=1, device_id={"fs": f, "tp": other}, device_id_type=MESH)
-    pl.semaphore_wait(barrier, nz + 2)
+    to_d = {"fs": zmate * Y_SIZE + y, "tp": xmate}
+    pl.semaphore_signal(barrier, inc=1, device_id=to_d, device_id_type=MESH)
+    pl.semaphore_wait(barrier, nz + 3)
 
     sent = []
 
@@ -240,11 +244,16 @@
             device_id_type=MESH,
         ).wait_recv()
 
-    def spread_z(g):
-        for d in range(1, 2 if g < 3 else nz):
+    def spread_z(g, outer=None, far=range(1, nz), held=None):
+        for d in (1,) if g < 3 else far:
             for way in (0, 1):
                 zt = z + d if way == 0 else z - d
                 exists = zt <= last if way == 0 else zt >= 0
+                if outer is not None:
+                    to_end = (zt == 0) | (zt == last)
+                    exists = exists & (to_end if outer else jnp.logical_not(to_end))
+                if held is not None:
+                    exists = exists & (at_end if held else jnp.logical_not(at_end))
                 start(exists, z_copy(g, source(g, lax.rem(zt + nz, 2)), z, zt, (d - 1) * 2 + way))
 
     def own(g):
@@ -255,11 +264,18 @@
             zs = z - d if way == 0 else z + d
             exists = zs >= 0 if way == 0 else zs <= last
             pl.when(exists)(functools.partial(take, g, zs, y))
-            if g < 3 and d < last:
+            if d < last:
                 onward = z < last if way == 0 else z > 0
                 zt = z + 1 if way == 0 else z - 1
                 start(exists & onward, z_copy(g, slot(g, zs, y), zs, zt, d * 2 + way))
             start(exists, y_copy(g, slot(g, zs, y), zs))
+
+    side = z // (nz // 2)
+    origins = [zmate] + [rank + side * (last - 2 * rank) for rank in range(2, nz)]
+
+    def hand_over(g, k):
+        take(g, origins[k], y)
+        start(None, y_copy(g, slot(g, origins[k], y), origins[k]))
 
     def take_across(g):
         for zs in range(nz):
@@ -310,19 +326,15 @@
 
     forward(0, 1)
     forward(1, 1)
-    spread_z(2)
     forward(0, 2)
     own(2)
     forward(1, 2)
+    spread_z(2)
     forward(0, 3)
     forward(1, 3)
     forward(2, 1)
-    forward(2, 2)
-    spread_z(3)
-    own(3)
-    forward(2, 3)
-    spread_z(4)
-    spread_z(5)
+    spread_z(3, False)
+    spread_z(4, False)
     for copy in stays:
         copy.wait()
     take_across(0)
@@ -349,15 +361,20 @@
         if 2 * by < rows:
             keep = keep * shifted_down(keep, by, 1.0)
         by *= 2
+    forward(2, 2)
     take_across(1)
     gate = jnp.dot(normed[...], fg[...], preferred_element_type=jnp.float32)
     gate = gate.astype(jnp.bfloat16).astype(jnp.float32)
     recurrent = (memory * jax.nn.gelu(gate)).astype(jnp.bfloat16)
 
+    forward(2, 3)
+    spread_z(3, True)
+    spread_z(4, True)
+    spread_z(5, False, held=False)
+    spread_z(6, False, held=False)
+    own(3)
     own(4)
-    forward(3, 1)
-
-    side = z // (nz // 2)
+
     inner = z + side * (last - 2 * z)
     ranks = [inner, 1 - inner] + list(range(2, nz))
     order = [rank + side * (last - 2 * rank) for rank in ranks]
@@ -384,21 +401,20 @@
         res[:, at] = (tok[own_at, at].astype(jnp.float32) + mixed).astype(jnp.bfloat16)
 
     for j in range(MIX_GROUPS):
+        if j == 2:
+            mix_first(1)
         take(2, order[j], 1 - y)
         product = contract_columns(recurrent, fo[mix_columns(j), :])
         part1[j] = product.astype(jnp.bfloat16).reshape(2, 2, own_rows, span)
         firsts.append(
             near_copy(part1.at[j, :, 1 - c], pair1.at[j], to_c, j, r_send, r_recv)
         )
-        if j > 0:
-            mix_first(j - 1)
+        if j == 1:
+            mix_first(0)
         if j > 1:
-            mix_second(j - 2)
-    mix_first(MIX_GROUPS - 1)
-    forward(4, 1)
-    forward(3, 2)
-    mix_second(MIX_GROUPS - 2)
-    mix_second(MIX_GROUPS - 1)
+            mix_first(j)
+    for j in range(MIX_GROUPS):
+        mix_second(j)
 
     mid[parity, t] = rms_scaled(res[...], scale2[...])
     mine = mid.at[parity, t]
@@ -406,10 +422,12 @@
     near_copy(mine, mine, to_x, 1, a_send, a_recv)
     near_copy(mine, mine, to_z, 0, a_send, a_recv)
     near_copy(mine, mine, to_c, 2, a_send, a_recv)
-    spread_z(6)
-
-    def arrived(par, who, index):
-        here = mid.at[par, who]
+    spread_z(5, False, held=True)
+    spread_z(6, False, held=True)
+    spread_z(5, True, (1,))
+    spread_z(6, True, (1,))
+
+    def arrived(here, index):
         pltpu.make_async_remote_copy(
             src_ref=here,
             dst_ref=here,
@@ -418,21 +436,27 @@
             device_id=to_c,
             device_id_type=MESH,
         ).wait_recv()
-        return here
-
-    forward(4, 2)
-    forward(3, 3)
-    forward(4, 3)
+
+    def pass_on(here, device, index):
+        near_copy(here, here, device, index, a_send, a_recv)
+
+    beside = mid.at[parity, xmate]
+    across = mid.at[1 - parity, xmate]
+    for k in range(nz - 1):
+        hand_over(3, k)
+    for k in range(nz - 1):
+        hand_over(4, k)
     own(5)
-    arrived(1 - parity, t, 0)
-    near_copy(theirs, theirs, to_x, 3, a_send, a_recv)
-    near_copy(theirs, theirs, to_c, 4, a_send, a_recv)
-    beside = arrived(parity, xmate, 1)
-    near_copy(beside, beside, to_c, 5, a_send, a_recv)
     own(6)
-    forward(5, 1)
-    arrived(parity, cmate, 2)
-    arrived(parity, diagonal, 5)
+    arrived(beside, 1)
+    pass_on(beside, to_c, 5)
+    arrived(theirs, 0)
+    pass_on(theirs, to_x, 3)
+    pass_on(theirs, to_c, 4)
+    spread_z(5, True, range(2, nz))
+    spread_z(6, True, range(2, nz))
+    arrived(mid.at[parity, cmate], 2)
+    arrived(mid.at[parity, diagonal], 5)
     take_across(3)
     take_across(4)
 
@@ -450,58 +474,100 @@
         lax.fori_loop(0, units // tile, up_tile, 0)
 
     up(parity)
-    forward(6, 1)
-    forward(5, 2)
-    beside = arrived(1 - parity, xmate, 3)
-    near_copy(beside, beside, to_c, 6, a_send, a_recv)
-    arrived(1 - parity, cmate, 4)
-    arrived(1 - parity, diagonal, 6)
+    hand_over(5, 0)
+    arrived(across, 3)
+    pass_on(across, to_c, 6)
+    arrived(mid.at[1 - parity, cmate], 4)
+    arrived(mid.at[1 - parity, diagonal], 6)
     up(1 - parity)
 
     narrow = width // DOWN_GROUPS
     exchanges = [[], [], []]
 
+    turns = [(1, 0), (0, 0), (1, 1), (0, 1)]
+    turns += [(rank, k) for k in range(2) for rank in range(2, nz)]
+
     def place(j):
-        return j // 2 + side * (last - 2 * (j // 2))
-
-    def down_first(j):
-        exchanges[0][j].wait_recv()
-        for par in range(2):
-            away = part2[j, par, 1 - x, c].astype(jnp.float32)
-            away = away + pair2[j, par, 1 - x].astype(jnp.float32)
-            xgive[j, par] = away.astype(jnp.bfloat16)
-        exchanges[1].append(
-            near_copy(xgive.at[j], xgot.at[j], to_x, DOWN_GROUPS + j, b_send, b_recv)
-        )
-
-    def partial_sum(j, par):
-        total = part2[j, par, x, c].astype(jnp.float32) + pair2[j, par, x].astype(jnp.float32)
-        return total + xgot[j, par].astype(jnp.float32)
-
-    def down_second(j):
-        exchanges[1][j].wait_recv()
-        zgive[j] = partial_sum(j, 1 - parity).astype(jnp.bfloat16)
-        exchanges[2].append(
-            near_copy(zgive.at[j], zgot.at[j], to_z, 2 * DOWN_GROUPS + j, b_send, b_recv)
-        )
-
-    def down_third(j):
-        exchanges[2][j].wait_recv()
-        total = partial_sum(j, parity) + zgot[j].astype(jnp.float32)
+        rank = turns[j][0]
+        return rank + side * (last - 2 * rank)
+
+    def pair_sum(j, par, xs):
+        return part2[j, par, xs, c].astype(jnp.float32) + pair2[j, par, xs].astype(jnp.float32)
+
+    def x_first(j):
+        return j not in (4, 6)
+
+    def down_out(j, total):
         for ys in range(Y_SIZE):
-            first = (place(j) * Y_SIZE + ys) * depth + (j % 2) * half
+            first = (place(j) * Y_SIZE + ys) * depth + turns[j][1] * half
             at = pl.ds(pl.multiple_of(first, half), half)
             out[:, at] = (
                 res[:, at].astype(jnp.float32) + total[:, ys * half : (ys + 1) * half]
             ).astype(jnp.bfloat16)
 
-    ahead = {0: [(6, 2), (5, 3)], 1: [(6, 3)]}
+    def down_direct(j):
+        exchanges[0][j].wait_recv()
+        agive[j, 0] = pair_sum(j, parity, 1 - x).astype(jnp.bfloat16)
+        agive[j, 1] = pair_sum(j, 1 - parity, x).astype(jnp.bfloat16)
+        bgive[j] = pair_sum(j, 1 - parity, 1 - x).astype(jnp.bfloat16)
+        trio = [
+            (bgive.at[j], bgot.at[j], to_d, 3),
+            (agive.at[j, 0], agot.at[j, 0], to_x, 1),
+            (agive.at[j, 1], agot.at[j, 1], to_z, 2),
+        ]
+        exchanges[1].append(
+            [near_copy(a, b, dev, k * DOWN_GROUPS + j, b_send, b_recv) for a, b, dev, k in trio]
+        )
+
+    def down_last(j):
+        for copy in exchanges[1][j]:
+            copy.wait_recv()
+        total = pair_sum(j, parity, x) + bgot[j].astype(jnp.float32)
+        total = total + agot[j, 0].astype(jnp.float32) + agot[j, 1].astype(jnp.float32)
+        down_out(j, total)
+
+    def down_first(j):
+        if j in DIRECT:
+            return down_direct(j)
+        exchanges[0][j].wait_recv()
+        for k in range(2):
+            away = pair_sum(j, k, 1 - x) if x_first(j) else pair_sum(j, 1 - parity, k)
+            agive[j, k] = away.astype(jnp.bfloat16)
+        device = to_x if x_first(j) else to_z
+        exchanges[1].append(
+            near_copy(agive.at[j], agot.at[j], device, DOWN_GROUPS + j, b_send, b_recv)
+        )
+
+    def down_second(j):
+        if j in DIRECT:
+            exchanges[2].append(None)
+            return
+        exchanges[1][j].wait_recv()
+        if x_first(j):
+            total = pair_sum(j, 1 - parity, x) + agot[j, 1 - parity].astype(jnp.float32)
+        else:
+            total = pair_sum(j, parity, 1 - x) + agot[j, 1 - x].astype(jnp.float32)
+        bgive[j] = total.astype(jnp.bfloat16)
+        device = to_z if x_first(j) else to_x
+        exchanges[2].append(
+            near_copy(bgive.at[j], bgot.at[j], device, 2 * DOWN_GROUPS + j, b_send, b_recv)
+        )
+
+    def down_third(j):
+        if j in DIRECT:
+            return down_last(j)
+        exchanges[2][j].wait_recv()
+        total = pair_sum(j, parity, x) + bgot[j].astype(jnp.float32)
+        total = total + agot[j, parity if x_first(j) else x].astype(jnp.float32)
+        down_out(j, total)
+
+    ahead = {0: [(6, 0)], 1: [(5, 1)], 2: [(5, 2)], 3: [(6, 1)], 4: [(6, 2)]}
     for j in range(DOWN_GROUPS):
-        for g, d in ahead.get(j, []):
-            forward(g, d)
+        for step in ahead.get(j, []):
+            hand_over(*step)
         q = place(j)
-        take(5 + j % 2, q, 1 - y)
-        at = pl.ds(pl.multiple_of((q * 2 + j % 2) * narrow, narrow), narrow)
+        take(5 + turns[j][1], q, 1 - y)
+        at = pl.ds(pl.multiple_of((q * 2 + turns[j][1]) * narrow, narrow), narrow)
         product = contract_columns(hidden[...].reshape(2 * rows, units), fd[at, :])
         part2[j] = product.astype(jnp.bfloat16).reshape(2, 2, 2, own_rows, narrow)
         exchanges[0].append(
@@ -509,16 +575,17 @@
         )
         if j > 0:
             down_first(j - 1)
-        if j > 1:
-            down_second(j - 2)
         if j > 2:
-            down_third(j - 3)
+            down_second(j - 3)
+        if j > 5:
+            down_third(j - 6)
     down_first(DOWN_GROUPS - 1)
+    down_second(DOWN_GROUPS - 3)
     down_second(DOWN_GROUPS - 2)
-    down_third(DOWN_GROUPS - 3)
+    down_third(DOWN_GROUPS - 6)
     down_second(DOWN_GROUPS - 1)
-    down_third(DOWN_GROUPS - 2)
-    down_third(DOWN_GROUPS - 1)
+    for j in range(DOWN_GROUPS - 5, DOWN_GROUPS):
+        down_third(j)
 
     for pred, copy in sent:
         if pred is None:
@@ -587,10 +654,10 @@
             pltpu.SemaphoreType.DMA((7, n_fs)),
             pltpu.SemaphoreType.DMA((2 * MIX_GROUPS,)),
             pltpu.SemaphoreType.DMA((2 * MIX_GROUPS,)),
-            pltpu.SemaphoreType.DMA((7,)),
-            pltpu.SemaphoreType.DMA((7,)),
-            pltpu.SemaphoreType.DMA((3 * DOWN_GROUPS,)),
-            pltpu.SemaphoreType.DMA((3 * DOWN_GROUPS,)),
+            pltpu.SemaphoreType.DMA((9,)),
+            pltpu.SemaphoreType.DMA((9,)),
+            pltpu.SemaphoreType.DMA((4 * DOWN_GROUPS,)),
+            pltpu.SemaphoreType.DMA((4 * DOWN_GROUPS,)),
             pltpu.SemaphoreType.DMA((9,)),
         ],
         compiler_params=pltpu.CompilerParams(

time: 113 us -> 102 us (0.903)
  Pallas kernels: 111 us -> 100 us
    pallas_call x1, Pallas kernels: 111 us -> 100 us  [fused_local(): pl.pallas_call(functools.partial(fused, n_fs // Y_SIZE), out_shape=jax.Sh...]
where the time goes in v2:
time: 102 us
  Pallas kernels  100 us (98%)
  local copies, waits for them, and re-layouts  1.77 us (2%)
    pallas_call x1, Pallas kernels, fused_local(): pl.pallas_call(functools.partial(fused, n_fs // Y_SIZE), out_shape=jax.Sh...  100 us

profile of v2, /device:TPU:0, one launch (start us, length us, event | category | flops | bytes accessed | tf_op | source)
XLA Modules:
  0.0 101.9 jit_solution(7290352018773703305)
XLA Ops:
  0.0 100.1 %fused_layer.1 = bf16[96,2048]{1,0:T(8,128)(2,1)} custom-call(bf16[384,2048]{1,0:T(8,128)(2,1)} %tok_in.1, f32[1,2048]{1,0:T(1,128)} %bitcast.3, bf16[256,256]{1,0:T(8,128)(2,1)} %wb.1, bf16[256,256]{1,0:T(8,128)(2,1)} %wg.1, bf16[4,256]{1,0:T(4,128)(2,1)} %taps.1, bf16[4,64,64]{2,1,0:T(8,128)(2,1)} %rblk.1, bf16[4,64,64]{2,1,0:T(8,128)(2,1)} %iblk.1, ...), custom_call_target="tpu_custom_call" | custom-call | tf_op jit(solution)/shard_map/fused_layer/pallas_call | solution.py:623
  100.1 1.8 %copy.15 = bf16[96,2048]{1,0:T(8,128)(2,1)} copy(bf16[96,2048]{1,0:T(8,128)(2,1)} %fused_layer.1) | data formatting | bytes 786432

commit v3 on v2

--- a/solution.py
+++ b/solution.py
@@ -116,7 +116,6 @@
 Y_SIZE = 2
 MIX_GROUPS = 4
 DOWN_GROUPS = 8
-DIRECT = (7,)
 
 
 def fits(mesh):
@@ -141,12 +140,13 @@
 
 def fused(
     nz,
-    tok_in, scale1, wb, wg, taps, rblk, iblk, logits, extra_in, wo, scale2, wu, wd,
-    out,
+    tok_in, scale1_in, wb, wg, taps_in, rblk_in, iblk_in, logits_in, extra_in, wo, scale2_in, wu, wd,
+    result,
+    scale1, taps, rblk, iblk, logits, scale2,
     normed, fb, fg, fo, fu, fd, rdiag, idiag, tok, extra,
     part1, pair1, give1, got1, res, mid, hidden,
-    part2, pair2, agive, agot, bgive, bgot,
-    z_send, y_send, w_recv, r_send, r_recv, a_send, a_recv, b_send, b_recv, l_sem,
+    part2, pair2, give2, got2, tally,
+    s_sem, along, lump, across, r_recv, a_recv, b_recv, l_sem,
 ):
     f = lax.axis_index("fs")
     t = lax.axis_index("tp")
@@ -161,39 +161,58 @@
     cmate = x * 2 + (1 - c)
     diagonal = (1 - x) * 2 + (1 - c)
     rows, width = tok.shape
-    own_rows = out.shape[0]
+    own_rows = result.shape[0]
     depth = wb.shape[0]
     half = depth // 2
     units = fu.shape[1]
 
+    barrier = pltpu.get_barrier_semaphore()
+
+    def greet(sem, device):
+        pl.semaphore_signal(sem, inc=1, device_id=device, device_id_type=MESH)
+
+    to_x = {"fs": f, "tp": xmate}
+    to_c = {"fs": f, "tp": cmate}
+    to_z = {"fs": zmate * Y_SIZE + y, "tp": t}
+    to_d = {"fs": zmate * Y_SIZE + y, "tp": xmate}
+    inside = jnp.logical_not(at_end)
+    for k in range(1, nz):
+        greet(barrier, {"fs": lax.rem(z + k, nz) * Y_SIZE + y, "tp": t})
+    for device in ({"fs": ymate, "tp": t}, to_x, to_c, to_d):
+        greet(barrier, device)
     early = [
-        pltpu.make_async_copy(tok_in, tok, l_sem.at[0]),
-        pltpu.make_async_copy(extra_in, extra, l_sem.at[1]),
+        pltpu.make_async_copy(given, kept, l_sem.at[1 + i])
+        for i, (given, kept) in enumerate(
+            (
+                (tok_in, tok),
+                (scale1_in, scale1),
+                (rblk_in, rblk),
+                (iblk_in, iblk),
+                (taps_in, taps),
+                (logits_in, logits),
+                (extra_in, extra),
+                (scale2_in, scale2),
+            )
+        )
     ]
+
     for copy in early:
         copy.start()
-    barrier = pltpu.get_barrier_semaphore()
-    for k in range(1, nz):
-        other = lax.rem(z + k, nz) * Y_SIZE + y
-        pl.semaphore_signal(barrier, inc=1, device_id={"fs": other, "tp": t}, device_id_type=MESH)
-    pl.semaphore_signal(barrier, inc=1, device_id={"fs": ymate, "tp": t}, device_id_type=MESH)
-    for other in (xmate, cmate):
-        pl.semaphore_signal(barrier, inc=1, device_id={"fs": f, "tp": other}, device_id_type=MESH)
-    to_d = {"fs": zmate * Y_SIZE + y, "tp": xmate}
-    pl.semaphore_signal(barrier, inc=1, device_id=to_d, device_id_type=MESH)
     pl.semaphore_wait(barrier, nz + 3)
-
-    sent = []
 
     def start(pred, copy):
         if pred is None:
             copy.start()
         else:
             pl.when(pred)(copy.start)
-        sent.append((pred, copy))
+
+    def settle(count, sem):
+        lot = tally.at[pl.ds(0, count * 16), :]
+        pltpu.make_async_copy(lot, lot, sem).wait()
 
     plain = (wb, wg, wo)
     whole = (fb, fg, fo)
+    lumped, single = (0, 1, 3, 4), (2, 5, 6)
 
     def source(g, way_parity):
         if g < 3:
@@ -213,12 +232,15 @@
         at = ((zs * 2 + (g - 5)) * Y_SIZE + ys) * half
         return fd.at[pl.ds(pl.multiple_of(at, half), half), :]
 
-    def z_copy(g, src, zs, zt, index):
+    def over(g, zs):
+        return lump.at[lumped.index(g)] if g in lumped else across.at[single.index(g), zs]
+
+    def z_copy(g, src, zs, zt):
         return pltpu.make_async_remote_copy(
             src_ref=src,
             dst_ref=slot(g, zs, y),
-            send_sem=z_send.at[g, index],
-            recv_sem=w_recv.at[g, zs * Y_SIZE + y],
+            send_sem=s_sem.at[0 if g < 3 else 1],
+            recv_sem=along.at[g, zs],
             device_id={"fs": zt * Y_SIZE + y, "tp": t},
             device_id_type=MESH,
         )
@@ -227,22 +249,17 @@
         return pltpu.make_async_remote_copy(
             src_ref=src,
             dst_ref=slot(g, zs, y),
-            send_sem=y_send.at[g, zs],
-            recv_sem=w_recv.at[g, zs * Y_SIZE + y],
+            send_sem=s_sem.at[2],
+            recv_sem=over(g, zs),
             device_id={"fs": ymate, "tp": t},
             device_id_type=MESH,
         )
 
-    def take(g, zs, ys):
-        here = slot(g, zs, ys)
-        pltpu.make_async_remote_copy(
-            src_ref=here,
-            dst_ref=here,
-            send_sem=y_send.at[g, zs],
-            recv_sem=w_recv.at[g, zs * Y_SIZE + ys],
-            device_id={"fs": ymate, "tp": t},
-            device_id_type=MESH,
-        ).wait_recv()
+    def landed(here, sem):
+        pltpu.make_async_copy(here, here, sem).wait()
+
+    def take(g, zs):
+        landed(slot(g, zs, y), along.at[g, zs])
 
     def spread_z(g, outer=None, far=range(1, nz), held=None):
         for d in (1,) if g < 3 else far:
@@ -254,7 +271,7 @@
                     exists = exists & (to_end if outer else jnp.logical_not(to_end))
                 if held is not None:
                     exists = exists & (at_end if held else jnp.logical_not(at_end))
-                start(exists, z_copy(g, source(g, lax.rem(zt + nz, 2)), z, zt, (d - 1) * 2 + way))
+                start(exists, z_copy(g, source(g, lax.rem(zt + nz, 2)), z, zt))
 
     def own(g):
         start(None, y_copy(g, source(g, parity), z))
@@ -263,40 +280,38 @@
         for way in (0, 1):
             zs = z - d if way == 0 else z + d
             exists = zs >= 0 if way == 0 else zs <= last
-            pl.when(exists)(functools.partial(take, g, zs, y))
+            pl.when(exists)(functools.partial(take, g, zs))
             if d < last:
                 onward = z < last if way == 0 else z > 0
                 zt = z + 1 if way == 0 else z - 1
-                start(exists & onward, z_copy(g, slot(g, zs, y), zs, zt, d * 2 + way))
+                start(exists & onward, z_copy(g, slot(g, zs, y), zs, zt))
             start(exists, y_copy(g, slot(g, zs, y), zs))
 
     side = z // (nz // 2)
     origins = [zmate] + [rank + side * (last - 2 * rank) for rank in range(2, nz)]
 
     def hand_over(g, k):
-        take(g, origins[k], y)
+        take(g, origins[k])
         start(None, y_copy(g, slot(g, origins[k], y), origins[k]))
 
-    def take_across(g):
-        for zs in range(nz):
-            take(g, zs, 1 - y)
-
-    def near_copy(src, dst, device, index, send, recv):
+    def take_lump(g):
+        count = nz * depth if g < 3 else nz * half
+        landed((whole[g] if g < 3 else fu).at[pl.ds(0, count), :], over(g, 0))
+
+    def take_over(g, zs):
+        landed(slot(g, zs, 1 - y), over(g, zs))
+
+    def near_copy(src, dst, device, sem):
         copy = pltpu.make_async_remote_copy(
             src_ref=src,
             dst_ref=dst,
-            send_sem=send.at[index],
-            recv_sem=recv.at[index],
+            send_sem=s_sem.at[3],
+            recv_sem=sem,
             device_id=device,
             device_id_type=MESH,
         )
         copy.start()
-        sent.append((None, copy))
         return copy
-
-    to_x = {"fs": f, "tp": xmate}
-    to_c = {"fs": f, "tp": cmate}
-    to_z = {"fs": zmate * Y_SIZE + y, "tp": t}
 
     spread_z(0)
     own(0)
@@ -304,18 +319,17 @@
     own(1)
 
     stays = [
-        pltpu.make_async_copy(source(g, parity), slot(g, z, y), l_sem.at[2 + g]) for g in range(7)
+        pltpu.make_async_copy(source(g, parity), slot(g, z, y), l_sem.at[0]) for g in range(7)
     ]
     for copy in stays:
         copy.start()
+    for copy in early:
+        copy.wait()
     block = rblk.shape[1]
     for blocks, diag in ((rblk, rdiag), (iblk, idiag)):
         diag[...] = jnp.zeros_like(diag)
         for b in range(rblk.shape[0]):
             diag[b * block : (b + 1) * block, b * block : (b + 1) * block] = blocks[b]
-
-    for copy in early:
-        copy.wait()
 
     def norm_rows(i, carry):
         at = pl.ds(pl.multiple_of(i * 32, 32), 32)
@@ -335,9 +349,8 @@
     forward(2, 1)
     spread_z(3, False)
     spread_z(4, False)
-    for copy in stays:
-        copy.wait()
-    take_across(0)
+    settle(depth // 16 * 7, l_sem.at[0])
+    take_lump(0)
 
     branch = jnp.dot(normed[...], fb[...], preferred_element_type=jnp.float32)
     branch = branch.astype(jnp.bfloat16).astype(jnp.float32)
@@ -362,7 +375,7 @@
             keep = keep * shifted_down(keep, by, 1.0)
         by *= 2
     forward(2, 2)
-    take_across(1)
+    take_lump(1)
     gate = jnp.dot(normed[...], fg[...], preferred_element_type=jnp.float32)
     gate = gate.astype(jnp.bfloat16).astype(jnp.float32)
     recurrent = (memory * jax.nn.gelu(gate)).astype(jnp.bfloat16)
@@ -390,7 +403,7 @@
         away = part1[j, 1 - x, c].astype(jnp.float32) + pair1[j, 1 - x].astype(jnp.float32)
         give1[j] = away.astype(jnp.bfloat16)
         seconds.append(
-            near_copy(give1.at[j], got1.at[j], to_x, MIX_GROUPS + j, r_send, r_recv)
+            near_copy(give1.at[j], got1.at[j], to_x, r_recv.at[MIX_GROUPS + j])
         )
 
     def mix_second(j):
@@ -403,11 +416,11 @@
     for j in range(MIX_GROUPS):
         if j == 2:
             mix_first(1)
-        take(2, order[j], 1 - y)
+        take_over(2, order[j])
         product = contract_columns(recurrent, fo[mix_columns(j), :])
         part1[j] = product.astype(jnp.bfloat16).reshape(2, 2, own_rows, span)
         firsts.append(
-            near_copy(part1.at[j, :, 1 - c], pair1.at[j], to_c, j, r_send, r_recv)
+            near_copy(part1.at[j, :, 1 - c], pair1.at[j], to_c, r_recv.at[j])
         )
         if j == 1:
             mix_first(0)
@@ -419,29 +432,22 @@
     mid[parity, t] = rms_scaled(res[...], scale2[...])
     mine = mid.at[parity, t]
     theirs = mid.at[1 - parity, t]
-    near_copy(mine, mine, to_x, 1, a_send, a_recv)
-    near_copy(mine, mine, to_z, 0, a_send, a_recv)
-    near_copy(mine, mine, to_c, 2, a_send, a_recv)
+    near_copy(mine, mine, to_x, a_recv.at[1])
+    near_copy(mine, mine, to_z, a_recv.at[0])
+    near_copy(mine, mine, to_c, a_recv.at[2])
     spread_z(5, False, held=True)
     spread_z(6, False, held=True)
     spread_z(5, True, (1,))
     spread_z(6, True, (1,))
 
     def arrived(here, index):
-        pltpu.make_async_remote_copy(
-            src_ref=here,
-            dst_ref=here,
-            send_sem=a_send.at[index],
-            recv_sem=a_recv.at[index],
-            device_id=to_c,
-            device_id_type=MESH,
-        ).wait_recv()
+        landed(here, a_recv.at[index])
 
     def pass_on(here, device, index):
-        near_copy(here, here, device, index, a_send, a_recv)
+        near_copy(here, here, device, a_recv.at[index])
 
     beside = mid.at[parity, xmate]
-    across = mid.at[1 - parity, xmate]
+    askew = mid.at[1 - parity, xmate]
     for k in range(nz - 1):
         hand_over(3, k)
     for k in range(nz - 1):
@@ -457,8 +463,8 @@
     spread_z(6, True, range(2, nz))
     arrived(mid.at[parity, cmate], 2)
     arrived(mid.at[parity, diagonal], 5)
-    take_across(3)
-    take_across(4)
+    take_lump(3)
+    take_lump(4)
 
     tile = 256
 
@@ -475,123 +481,143 @@
 
     up(parity)
     hand_over(5, 0)
-    arrived(across, 3)
-    pass_on(across, to_c, 6)
+    arrived(askew, 3)
+    pass_on(askew, to_c, 6)
     arrived(mid.at[1 - parity, cmate], 4)
     arrived(mid.at[1 - parity, diagonal], 6)
     up(1 - parity)
 
     narrow = width // DOWN_GROUPS
-    exchanges = [[], [], []]
-
-    turns = [(1, 0), (0, 0), (1, 1), (0, 1)]
-    turns += [(rank, k) for k in range(2) for rank in range(2, nz)]
+    halves = [k for r in range(2) for k in range(2)] + [k for k in range(2) for r in range(2, nz)]
+    final = DOWN_GROUPS - 1
+    lots = [(j, None) for j in range(final - 1)] + [(final, 0), (final - 1, None), (final, 1)]
+    shared, spread = {}, {}
+    level = jnp.where(at_end, 0, 1)
+
+    def number(lot):
+        j, which = lot
+        if j >= 4:
+            return j + (which or 0)
+        return (level if j < 2 else 1 - level) * 2 + j % 2
 
     def place(j):
-        rank = turns[j][0]
+        if j < 4:
+            return z if j < 2 else zmate
+        rank = 2 + (j - 4) % (nz - 2)
         return rank + side * (last - 2 * rank)
 
-    def pair_sum(j, par, xs):
-        return part2[j, par, xs, c].astype(jnp.float32) + pair2[j, par, xs].astype(jnp.float32)
-
-    def x_first(j):
-        return j not in (4, 6)
-
-    def down_out(j, total):
-        for ys in range(Y_SIZE):
-            first = (place(j) * Y_SIZE + ys) * depth + turns[j][1] * half
+    def signal_at(lot, k):
+        return b_recv.at[number(lot), k]
+
+    def lot_columns(lot):
+        which = lot[1]
+        return pl.ds(0, narrow if which is None else half)
+
+    def lot_sides(lot):
+        which = lot[1]
+        return list(range(Y_SIZE)) if which is None else [y if which == 0 else 1 - y]
+
+    def pair_sum(lot, par, xs):
+        at = lot_columns(lot)
+        mine = part2[number(lot), par, xs, c, :, at].astype(jnp.float32)
+        return mine + pair2[number(lot), par, xs, :, at].astype(jnp.float32)
+
+    def multiply(i):
+        lot = lots[i]
+        j, which = lot
+        q = place(j)
+        if which != 0:
+            take_over(5 + halves[j], q)
+        first = (q * 2 + halves[j]) * narrow
+        if which is not None:
+            first = first + lot_sides(lot)[0] * half
+        at = lot_columns(lot)
+        some = fd[pl.ds(pl.multiple_of(first, half), at.size), :]
+        product = contract_columns(hidden[...].reshape(2 * rows, units), some)
+        n = number(lot)
+        part2[n, :, :, :, :, at] = product.astype(jnp.bfloat16).reshape(2, 2, 2, own_rows, at.size)
+        shared[lot] = near_copy(
+            part2.at[n, :, :, 1 - c, :, at], pair2.at[n, :, :, :, at], to_c, signal_at(lot, 0)
+        )
+
+    def exchange(i):
+        lot = lots[i]
+        shared[lot].wait_recv()
+        at = lot_columns(lot)
+        ways = [
+            (to_d, 1 - parity, 1 - x),
+            (to_x, parity, 1 - x),
+            (to_z, 1 - parity, x),
+        ]
+        spread[lot] = []
+        for k, (device, par, xs) in enumerate(ways):
+            n = number(lot)
+            give2[n, k, :, at] = pair_sum(lot, par, xs).astype(jnp.bfloat16)
+            spread[lot].append(
+                near_copy(
+                    give2.at[n, k, :, at], got2.at[n, k, :, at], device, signal_at(lot, k + 1)
+                )
+            )
+
+    def finish(i):
+        lot = lots[i]
+        for copy in spread[lot]:
+            copy.wait_recv()
+        total = pair_sum(lot, parity, x)
+        for k in range(3):
+            total = total + got2[number(lot), k, :, lot_columns(lot)].astype(jnp.float32)
+        for k, ys in enumerate(lot_sides(lot)):
+            first = (place(lot[0]) * Y_SIZE + ys) * depth + halves[lot[0]] * half
             at = pl.ds(pl.multiple_of(first, half), half)
-            out[:, at] = (
-                res[:, at].astype(jnp.float32) + total[:, ys * half : (ys + 1) * half]
+            result[:, at] = (
+                res[:, at].astype(jnp.float32) + total[:, k * half : (k + 1) * half]
             ).astype(jnp.bfloat16)
 
-    def down_direct(j):
-        exchanges[0][j].wait_recv()
-        agive[j, 0] = pair_sum(j, parity, 1 - x).astype(jnp.bfloat16)
-        agive[j, 1] = pair_sum(j, 1 - parity, x).astype(jnp.bfloat16)
-        bgive[j] = pair_sum(j, 1 - parity, 1 - x).astype(jnp.bfloat16)
-        trio = [
-            (bgive.at[j], bgot.at[j], to_d, 3),
-            (agive.at[j, 0], agot.at[j, 0], to_x, 1),
-            (agive.at[j, 1], agot.at[j, 1], to_z, 2),
-        ]
-        exchanges[1].append(
-            [near_copy(a, b, dev, k * DOWN_GROUPS + j, b_send, b_recv) for a, b, dev, k in trio]
-        )
-
-    def down_last(j):
-        for copy in exchanges[1][j]:
-            copy.wait_recv()
-        total = pair_sum(j, parity, x) + bgot[j].astype(jnp.float32)
-        total = total + agot[j, 0].astype(jnp.float32) + agot[j, 1].astype(jnp.float32)
-        down_out(j, total)
-
-    def down_first(j):
-        if j in DIRECT:
-            return down_direct(j)
-        exchanges[0][j].wait_recv()
-        for k in range(2):
-            away = pair_sum(j, k, 1 - x) if x_first(j) else pair_sum(j, 1 - parity, k)
-            agive[j, k] = away.astype(jnp.bfloat16)
-        device = to_x if x_first(j) else to_z
-        exchanges[1].append(
-            near_copy(agive.at[j], agot.at[j], device, DOWN_GROUPS + j, b_send, b_recv)
-        )
-
-    def down_second(j):
-        if j in DIRECT:
-            exchanges[2].append(None)
-            return
-        exchanges[1][j].wait_recv()
-        if x_first(j):
-            total = pair_sum(j, 1 - parity, x) + agot[j, 1 - parity].astype(jnp.float32)
-        else:
-            total = pair_sum(j, parity, 1 - x) + agot[j, 1 - x].astype(jnp.float32)
-        bgive[j] = total.astype(jnp.bfloat16)
-        device = to_z if x_first(j) else to_x
-        exchanges[2].append(
-            near_copy(bgive.at[j], bgot.at[j], device, 2 * DOWN_GROUPS + j, b_send, b_recv)
-        )
-
-    def down_third(j):
-        if j in DIRECT:
-            return down_last(j)
-        exchanges[2][j].wait_recv()
-        total = pair_sum(j, parity, x) + bgot[j].astype(jnp.float32)
-        total = total + agot[j, parity if x_first(j) else x].astype(jnp.float32)
-        down_out(j, total)
-
-    ahead = {0: [(6, 0)], 1: [(5, 1)], 2: [(5, 2)], 3: [(6, 1)], 4: [(6, 2)]}
-    for j in range(DOWN_GROUPS):
-        for step in ahead.get(j, []):
-            hand_over(*step)
-        q = place(j)
-        take(5 + turns[j][1], q, 1 - y)
-        at = pl.ds(pl.multiple_of((q * 2 + turns[j][1]) * narrow, narrow), narrow)
-        product = contract_columns(hidden[...].reshape(2 * rows, units), fd[at, :])
-        part2[j] = product.astype(jnp.bfloat16).reshape(2, 2, 2, own_rows, narrow)
-        exchanges[0].append(
-            near_copy(part2.at[j, :, :, 1 - c], pair2.at[j], to_c, j, b_send, b_recv)
-        )
-        if j > 0:
-            down_first(j - 1)
-        if j > 2:
-            down_second(j - 3)
-        if j > 5:
-            down_third(j - 6)
-    down_first(DOWN_GROUPS - 1)
-    down_second(DOWN_GROUPS - 3)
-    down_second(DOWN_GROUPS - 2)
-    down_third(DOWN_GROUPS - 6)
-    down_second(DOWN_GROUPS - 1)
-    for j in range(DOWN_GROUPS - 5, DOWN_GROUPS):
-        down_third(j)
-
-    for pred, copy in sent:
-        if pred is None:
-            copy.wait_send()
-        else:
-            pl.when(pred)(copy.wait_send)
+    plan = [
+        (hand_over, 6, 0),
+        (multiply, 0),
+        (multiply, 1),
+        (exchange, 0),
+        (exchange, 1),
+        (multiply, 2),
+        (hand_over, 5, 1),
+        (exchange, 2),
+        (hand_over, 5, 2),
+        (multiply, 3),
+        (exchange, 3),
+        (multiply, 4),
+        (exchange, 4),
+        (hand_over, 6, 1),
+        (multiply, 5),
+        (exchange, 5),
+        (hand_over, 6, 2),
+        (multiply, 6),
+        (exchange, 6),
+        (multiply, 7),
+        (exchange, 7),
+        (multiply, 8),
+        (exchange, 8),
+        (finish, 0),
+        (finish, 1),
+        (finish, 2),
+        (finish, 3),
+        (finish, 4),
+        (finish, 5),
+        (finish, 6),
+        (finish, 7),
+        (finish, 8),
+    ]
+    for step, *which in plan:
+        step(*which)
+    pl.when(at_end)(functools.partial(settle, depth // 16 * 3, s_sem.at[0]))
+    relayed = 3 * (2 + nz - 1)
+    pl.when(inside)(functools.partial(settle, depth // 16 * relayed, s_sem.at[0]))
+    settle(depth // 16 * 4 * (nz - 1), s_sem.at[1])
+    settle(depth // 16 * 7 * nz, s_sem.at[2])
+    bits = own_rows * width // (16 * depth)
+    mixed = own_rows * span // (16 * depth)
+    summed = own_rows * narrow // (16 * depth)
+    settle(7 * bits + 3 * MIX_GROUPS * mixed + 7 * DOWN_GROUPS * summed, s_sem.at[3])
 
 
 def fused_local(
@@ -618,14 +644,19 @@
     span = width // MIX_GROUPS
     narrow = width // DOWN_GROUPS
     low, high = jnp.bfloat16, jnp.float32
-    vmem = pl.BlockSpec(memory_space=pltpu.VMEM)
     hbm = pl.BlockSpec(memory_space=pl.ANY)
     return pl.pallas_call(
         functools.partial(fused, n_fs // Y_SIZE),
-        out_shape=jax.ShapeDtypeStruct((own_rows, width), low),
-        in_specs=[hbm, vmem, hbm, hbm] + [vmem] * 4 + [hbm, hbm, vmem, hbm, hbm],
-        out_specs=vmem,
+        out_shape=pltpu.VMEM((own_rows, width), low),
+        in_specs=[hbm] * 13,
+        out_specs=pl.BlockSpec(memory_space=pltpu.VMEM),
         scratch_shapes=[
+            pltpu.VMEM((1, width), high),
+            pltpu.VMEM(filter_taps_weight.shape, low),
+            pltpu.VMEM(recurrence_gate_blocks.shape, low),
+            pltpu.VMEM(input_gate_blocks.shape, low),
+            pltpu.VMEM((1, channels), high),
+            pltpu.VMEM((1, width), high),
             pltpu.VMEM((rows, width), low),
             pltpu.VMEM((width, channels), low),
             pltpu.VMEM((width, channels), low),
@@ -643,21 +674,18 @@
             pltpu.VMEM((own_rows, width), low),
             pltpu.VMEM((2, n_tp, own_rows, width), low),
             pltpu.VMEM((2, rows, units), low),
-            pltpu.VMEM((DOWN_GROUPS, 2, 2, 2, own_rows, narrow), low),
-            pltpu.VMEM((DOWN_GROUPS, 2, 2, own_rows, narrow), low),
-            pltpu.VMEM((DOWN_GROUPS, 2, own_rows, narrow), low),
-            pltpu.VMEM((DOWN_GROUPS, 2, own_rows, narrow), low),
-            pltpu.VMEM((DOWN_GROUPS, own_rows, narrow), low),
-            pltpu.VMEM((DOWN_GROUPS, own_rows, narrow), low),
-            pltpu.SemaphoreType.DMA((7, 6)),
+            pltpu.VMEM((DOWN_GROUPS + 1, 2, 2, 2, own_rows, narrow), low),
+            pltpu.VMEM((DOWN_GROUPS + 1, 2, 2, own_rows, narrow), low),
+            pltpu.VMEM((DOWN_GROUPS + 1, 3, own_rows, narrow), low),
+            pltpu.VMEM((DOWN_GROUPS + 1, 3, own_rows, narrow), low),
+            pltpu.VMEM((16 * 1024, width // 8), low),
+            pltpu.SemaphoreType.DMA((4,)),
             pltpu.SemaphoreType.DMA((7, n_fs // Y_SIZE)),
-            pltpu.SemaphoreType.DMA((7, n_fs)),
+            pltpu.SemaphoreType.DMA((4,)),
+            pltpu.SemaphoreType.DMA((3, n_fs // Y_SIZE)),
             pltpu.SemaphoreType.DMA((2 * MIX_GROUPS,)),
-            pltpu.SemaphoreType.DMA((2 * MIX_GROUPS,)),
-            pltpu.SemaphoreType.DMA((9,)),
-            pltpu.SemaphoreType.DMA((9,)),
-            pltpu.SemaphoreType.DMA((4 * DOWN_GROUPS,)),
-            pltpu.SemaphoreType.DMA((4 * DOWN_GROUPS,)),
+            pltpu.SemaphoreType.DMA((7,)),
+            pltpu.SemaphoreType.DMA((DOWN_GROUPS + 1, 4)),
             pltpu.SemaphoreType.DMA((9,)),
         ],
         compiler_params=pltpu.CompilerParams(

time: 102 us -> 96.7 us (0.948)
  Pallas kernels: 100 us -> 95.8 us
  local copies, waits for them, and re-layouts: 1.77 us -> 0.75 us
    pallas_call x1, Pallas kernels: 100 us -> 95.8 us  [fused_local(): pl.pallas_call(functools.partial(fused, n_fs // Y_SIZE), out_shape=pltpu....]
where the time goes in v3:
time: 96.7 us; the launch traced here: 96.6 us
  Pallas kernels  95.8 us (99%)
    pallas_call x1, Pallas kernels, fused_local(): pl.pallas_call(functools.partial(fused, n_fs // Y_SIZE), out_shape=pltpu....  95.8 us

profile of v3, /device:TPU:0, one launch (start us, length us, event | category | flops | bytes accessed | tf_op | source)
XLA Modules:
  0.0 96.6 jit_solution(15119629183727788624)
XLA Ops:
  0.0 95.8 %fused_layer.1 = bf16[96,2048]{1,0:T(8,128)(2,1)S(1)} custom-call(bf16[384,2048]{1,0:T(8,128)(2,1)} %tok_in.1, f32[1,2048]{1,0:T(1,128)} %bitcast.3, bf16[256,256]{1,0:T(8,128)(2,1)} %wb.1, bf16[256,256]{1,0:T(8,128)(2,1)} %wg.1, bf16[4,256]{1,0:T(4,128)(2,1)} %taps_in.1, bf16[4,64,64]{2,1,0:T(8,128)(2,1)} %rblk_in.1, bf16[4,64,64]{2,1,0:T(8,128)(2,1)} %iblk_in.1, ...), custom_call_target="tpu_custom_call" | custom-call | tf_op jit(solution)/shard_map/fused_layer/pallas_call | solution.py:648
  95.8 0.7 copy.15

commit v4 on v3

--- a/solution.py
+++ b/solution.py
@@ -116,6 +116,8 @@
 Y_SIZE = 2
 MIX_GROUPS = 4
 DOWN_GROUPS = 8
+STEPPED = (0, 1, 2, 3)
+X_FIRST = (0, 2)
 
 
 def fits(mesh):
@@ -273,8 +275,8 @@
                     exists = exists & (at_end if held else jnp.logical_not(at_end))
                 start(exists, z_copy(g, source(g, lax.rem(zt + nz, 2)), z, zt))
 
-    def own(g):
-        start(None, y_copy(g, source(g, parity), z))
+    def own(g, pred=None):
+        start(pred, y_copy(g, source(g, parity), z))
 
     def forward(g, d):
         for way in (0, 1):
@@ -290,9 +292,12 @@
     side = z // (nz // 2)
     origins = [zmate] + [rank + side * (last - 2 * rank) for rank in range(2, nz)]
 
-    def hand_over(g, k):
-        take(g, origins[k])
-        start(None, y_copy(g, slot(g, origins[k], y), origins[k]))
+    def hand_over(g, k, pred=None):
+        if pred is None:
+            take(g, origins[k])
+        else:
+            pl.when(pred)(functools.partial(take, g, origins[k]))
+        start(pred, y_copy(g, slot(g, origins[k], y), origins[k]))
 
     def take_lump(g):
         count = nz * depth if g < 3 else nz * half
@@ -387,6 +392,9 @@
     spread_z(6, False, held=False)
     own(3)
     own(4)
+    own(5, at_end)
+    hand_over(3, 1, inside)
+    hand_over(4, 1, inside)
 
     inner = z + side * (last - 2 * z)
     ranks = [inner, 1 - inner] + list(range(2, nz))
@@ -448,11 +456,10 @@
 
     beside = mid.at[parity, xmate]
     askew = mid.at[1 - parity, xmate]
-    for k in range(nz - 1):
-        hand_over(3, k)
-    for k in range(nz - 1):
-        hand_over(4, k)
-    own(5)
+    for g in (3, 4):
+        for k in range(nz - 1):
+            hand_over(g, k, at_end if k == 1 else None)
+    own(5, inside)
     own(6)
     arrived(beside, 1)
     pass_on(beside, to_c, 5)
@@ -544,6 +551,17 @@
         lot = lots[i]
         shared[lot].wait_recv()
         at = lot_columns(lot)
+        n = number(lot)
+        if i in STEPPED:
+            for k in range(2):
+                away = pair_sum(lot, k, 1 - x) if i in X_FIRST else pair_sum(lot, 1 - parity, k)
+                give2[n, k] = away.astype(jnp.bfloat16)
+            two = pl.ds(0, 2)
+            device = to_x if i in X_FIRST else to_z
+            spread[lot] = [
+                near_copy(give2.at[n, two], got2.at[n, two], device, signal_at(lot, 1))
+            ]
+            return
         ways = [
             (to_d, 1 - parity, 1 - x),
             (to_x, parity, 1 - x),
@@ -551,7 +569,6 @@
         ]
         spread[lot] = []
         for k, (device, par, xs) in enumerate(ways):
-            n = number(lot)
             give2[n, k, :, at] = pair_sum(lot, par, xs).astype(jnp.bfloat16)
             spread[lot].append(
                 near_copy(
@@ -559,12 +576,24 @@
                 )
             )
 
+    def pass_across(i):
+        lot = lots[i]
+        spread[lot][0].wait_recv()
+        n = number(lot)
+        if i in X_FIRST:
+            away = pair_sum(lot, 1 - parity, x) + got2[n, 1 - parity].astype(jnp.float32)
+        else:
+            away = pair_sum(lot, parity, 1 - x) + got2[n, 1 - x].astype(jnp.float32)
+        give2[n, 2] = away.astype(jnp.bfloat16)
+        device = to_z if i in X_FIRST else to_x
+        spread[lot] = [near_copy(give2.at[n, 2], got2.at[n, 2], device, signal_at(lot, 2))]
+
     def finish(i):
         lot = lots[i]
         for copy in spread[lot]:
             copy.wait_recv()
         total = pair_sum(lot, parity, x)
-        for k in range(3):
+        for k in [parity if i in X_FIRST else x, 2] if i in STEPPED else range(3):
             total = total + got2[number(lot), k, :, lot_columns(lot)].astype(jnp.float32)
         for k, ys in enumerate(lot_sides(lot)):
             first = (place(lot[0]) * Y_SIZE + ys) * depth + halves[lot[0]] * half
@@ -585,16 +614,20 @@
         (hand_over, 5, 2),
         (multiply, 3),
         (exchange, 3),
+        (hand_over, 6, 1),
         (multiply, 4),
+        (pass_across, 0),
         (exchange, 4),
-        (hand_over, 6, 1),
+        (hand_over, 6, 2),
         (multiply, 5),
+        (pass_across, 1),
         (exchange, 5),
-        (hand_over, 6, 2),
         (multiply, 6),
         (exchange, 6),
+        (pass_across, 2),
         (multiply, 7),
         (exchange, 7),
+        (pass_across, 3),
         (multiply, 8),
         (exchange, 8),
         (finish, 0),

time: 96.7 us -> 95 us (0.982)
  Pallas kernels: 95.8 us -> 94.1 us
    pallas_call x1, Pallas kernels: 95.8 us -> 94.1 us  [fused_local(): pl.pallas_call(functools.partial(fused, n_fs // Y_SIZE), out_shape=pltpu....]
where the time goes in v4:
time: 95 us; the launch traced here: 94.9 us
  Pallas kernels  94.1 us (99%)
    pallas_call x1, Pallas kernels, fused_local(): pl.pallas_call(functools.partial(fused, n_fs // Y_SIZE), out_shape=pltpu....  94.1 us

profile of v4, /device:TPU:0, one launch (start us, length us, event | category | flops | bytes accessed | tf_op | source)
XLA Modules:
  0.0 94.9 jit_solution(9976405039837917722)
XLA Ops:
  0.0 94.1 %fused_layer.1 = bf16[96,2048]{1,0:T(8,128)(2,1)S(1)} custom-call(bf16[384,2048]{1,0:T(8,128)(2,1)} %tok_in.1, f32[1,2048]{1,0:T(1,128)} %bitcast.3, bf16[256,256]{1,0:T(8,128)(2,1)} %wb.1, bf16[256,256]{1,0:T(8,128)(2,1)} %wg.1, bf16[4,256]{1,0:T(4,128)(2,1)} %taps_in.1, bf16[4,64,64]{2,1,0:T(8,128)(2,1)} %rblk_in.1, bf16[4,64,64]{2,1,0:T(8,128)(2,1)} %iblk_in.1, ...), custom_call_target="tpu_custom_call" | custom-call | tf_op jit(solution)/shard_map/fused_layer/pallas_call | solution.py:681
  94.1 0.7 copy.15

commit v5 on v4

--- a/solution.py
+++ b/solution.py
@@ -116,7 +116,7 @@
 Y_SIZE = 2
 MIX_GROUPS = 4
 DOWN_GROUPS = 8
-STEPPED = (0, 1, 2, 3)
+STEPPED = (0, 2)
 X_FIRST = (0, 2)
 
 
@@ -395,6 +395,7 @@
     own(5, at_end)
     hand_over(3, 1, inside)
     hand_over(4, 1, inside)
+    own(5, inside)
 
     inner = z + side * (last - 2 * z)
     ranks = [inner, 1 - inner] + list(range(2, nz))
@@ -459,7 +460,6 @@
     for g in (3, 4):
         for k in range(nz - 1):
             hand_over(g, k, at_end if k == 1 else None)
-    own(5, inside)
     own(6)
     arrived(beside, 1)
     pass_on(beside, to_c, 5)
@@ -620,23 +620,21 @@
         (exchange, 4),
         (hand_over, 6, 2),
         (multiply, 5),
-        (pass_across, 1),
         (exchange, 5),
+        (pass_across, 2),
         (multiply, 6),
         (exchange, 6),
-        (pass_across, 2),
         (multiply, 7),
         (exchange, 7),
-        (pass_across, 3),
         (multiply, 8),
         (exchange, 8),
+        (finish, 4),
+        (finish, 5),
+        (finish, 6),
         (finish, 0),
         (finish, 1),
         (finish, 2),
         (finish, 3),
-        (finish, 4),
-        (finish, 5),
-        (finish, 6),
         (finish, 7),
         (finish, 8),
     ]

time: 95 us -> 94.9 us (level)
  no operation moved by 1% of the time
where the time goes in v5:
time: 94.9 us; the launch traced here: 94.8 us
  Pallas kernels  94 us (99%)
    pallas_call x1, Pallas kernels, fused_local(): pl.pallas_call(functools.partial(fused, n_fs // Y_SIZE), out_shape=pltpu....  94 us

profile of v5, /device:TPU:0, one launch (start us, length us, event | category | flops | bytes accessed | tf_op | source)
XLA Modules:
  0.0 94.8 jit_solution(10587689227872948068)
XLA Ops:
  0.0 94.0 %fused_layer.1 = bf16[96,2048]{1,0:T(8,128)(2,1)S(1)} custom-call(bf16[384,2048]{1,0:T(8,128)(2,1)} %tok_in.1, f32[1,2048]{1,0:T(1,128)} %bitcast.3, bf16[256,256]{1,0:T(8,128)(2,1)} %wb.1, bf16[256,256]{1,0:T(8,128)(2,1)} %wg.1, bf16[4,256]{1,0:T(4,128)(2,1)} %taps_in.1, bf16[4,64,64]{2,1,0:T(8,128)(2,1)} %rblk_in.1, bf16[4,64,64]{2,1,0:T(8,128)(2,1)} %iblk_in.1, ...), custom_call_target="tpu_custom_call" | custom-call | tf_op jit(solution)/shard_map/fused_layer/pallas_call | solution.py:679
  94.0 0.7 copy.15

commit v6 on v5

--- a/solution.py
+++ b/solution.py
@@ -572,7 +572,7 @@
             give2[n, k, :, at] = pair_sum(lot, par, xs).astype(jnp.bfloat16)
             spread[lot].append(
                 near_copy(
-                    give2.at[n, k, :, at], got2.at[n, k, :, at], device, signal_at(lot, k + 1)
+                    give2.at[n, k, :, at], got2.at[n, k, :, at], device, signal_at(lot, 1)
                 )
             )
 
@@ -590,8 +590,10 @@
 
     def finish(i):
         lot = lots[i]
-        for copy in spread[lot]:
-            copy.wait_recv()
+        if i in STEPPED:
+            spread[lot][0].wait_recv()
+        else:
+            landed(got2.at[number(lot), :, :, lot_columns(lot)], signal_at(lot, 1))
         total = pair_sum(lot, parity, x)
         for k in [parity if i in X_FIRST else x, 2] if i in STEPPED else range(3):
             total = total + got2[number(lot), k, :, lot_columns(lot)].astype(jnp.float32)
@@ -716,7 +718,7 @@
             pltpu.SemaphoreType.DMA((3, n_fs // Y_SIZE)),
             pltpu.SemaphoreType.DMA((2 * MIX_GROUPS,)),
             pltpu.SemaphoreType.DMA((7,)),
-            pltpu.SemaphoreType.DMA((DOWN_GROUPS + 1, 4)),
+            pltpu.SemaphoreType.DMA((DOWN_GROUPS + 1, 3)),
             pltpu.SemaphoreType.DMA((9,)),
         ],
         compiler_params=pltpu.CompilerParams(

time: 94.9 us -> 94.8 us (level)
  no operation moved by 1% of the time
where the time goes in v6:
time: 94.8 us; the launch traced here: 94.7 us
  Pallas kernels  93.9 us (99%)
    pallas_call x1, Pallas kernels, fused_local(): pl.pallas_call(functools.partial(fused, n_fs // Y_SIZE), out_shape=pltpu....  93.9 us

profile of v6, /device:TPU:0, one launch (start us, length us, event | category | flops | bytes accessed | tf_op | source)
XLA Modules:
  0.0 94.7 jit_solution(9248689516035100524)
XLA Ops:
  0.0 93.9 %fused_layer.1 = bf16[96,2048]{1,0:T(8,128)(2,1)S(1)} custom-call(bf16[384,2048]{1,0:T(8,128)(2,1)} %tok_in.1, f32[1,2048]{1,0:T(1,128)} %bitcast.3, bf16[256,256]{1,0:T(8,128)(2,1)} %wb.1, bf16[256,256]{1,0:T(8,128)(2,1)} %wg.1, bf16[4,256]{1,0:T(4,128)(2,1)} %taps_in.1, bf16[4,64,64]{2,1,0:T(8,128)(2,1)} %rblk_in.1, bf16[4,64,64]{2,1,0:T(8,128)(2,1)} %iblk_in.1, ...), custom_call_target="tpu_custom_call" | custom-call | tf_op jit(solution)/shard_map/fused_layer/pallas_call | solution.py:681
  93.9 0.7 copy.15
